TPU v7x, 32 devices: a whole 2x2x4 slice. The times are simulated.
32 devices in a mesh: kv: 8 (over z, y), tp: 4 (over x, core).
Axes of the slice: x: 2, y: 2, z: 4, core: 2. Of those that a mesh axis runs over, the one named last changes fastest.
Arguments:
- tokens: bfloat16 [256, 4096], P(None, ('kv', 'tp')), may hold values from -60 to 60
- past_state: float32 [256, 16, 128, 128], P('kv', 'tp'), may hold values from -4 to 4
- pre_gain: float32 [4096], replicated, may hold values from 0.1 to 1.9
- pre_gate: bfloat16 [4096, 11264], P(None, ('kv', 'tp')), may hold values from -0.09375 to 0.09375
- pre_up: bfloat16 [4096, 11264], P(None, ('kv', 'tp')), may hold values from -0.09375 to 0.09375
- pre_down: bfloat16 [11264, 4096], P(('kv', 'tp')), may hold values from -0.109375 to 0.109375
- mix_gain: float32 [4096], replicated, may hold values from 0.1 to 1.9
- query_weight: bfloat16 [4096, 2048], P('kv', 'tp'), may hold values from -0.09375 to 0.09375
- forget_weight: bfloat16 [4096, 2048], P('kv', 'tp'), may hold values from -0.09375 to 0.09375
- value_weight: bfloat16 [4096, 2048], P('kv', 'tp'), may hold values from -0.09375 to 0.09375
- output_gate_weight: bfloat16 [4096, 2048], P('kv', 'tp'), may hold values from -0.09375 to 0.09375
- forget_floor: float32 [2048], P('tp'), may hold values from 0.02 to 0.9
- head_gain: float32 [128], replicated, may hold values from 0.1 to 1.9
- proj_out: bfloat16 [2048, 4096], P('tp', 'kv'), may hold values from -0.125 to 0.125
- post_gain: float32 [4096], replicated, may hold values from 0.1 to 1.9
- post_gate: bfloat16 [4096, 11264], P(None, ('kv', 'tp')), may hold values from -0.09375 to 0.09375
- post_up: bfloat16 [4096, 11264], P(None, ('kv', 'tp')), may hold values from -0.09375 to 0.09375
- post_down: bfloat16 [11264, 4096], P(('kv', 'tp')), may hold values from -0.109375 to 0.109375
Outputs:
- result: bfloat16 [256, 4096], P(None, ('kv', 'tp'))
- new_state: float32 [256, 16, 128, 128], P('kv', 'tp')
All inputs are finite; a program needn't handle non-finite values.
Results may differ from a plain program's by a relative error of at most 0.014.
Values may be sent and summed in bfloat16 or wider, within the bound.
A program may use at most 128 MiB of HBM per device.

v0:
```python
import functools

import jax
import jax.numpy as jnp
from jax import lax
from jax.experimental import pallas as pl
from jax.experimental.pallas import tpu as pltpu
from jax.sharding import PartitionSpec as P

D = 4096


epsilon = 1e-06


def half_inputs(activations, gain, w_gate, w_up):
    piece_float = lax.all_gather(activations, ("kv", "tp"), axis=1, tiled=True).astype(jnp.float32)
    normed = (piece_float * gain).astype(jnp.bfloat16)
    gate_acc = jnp.dot(normed, w_gate, preferred_element_type=jnp.float32)
    up_acc = jnp.dot(normed, w_up, preferred_element_type=jnp.float32)
    squares = jnp.sum(piece_float * piece_float, axis=1)
    row_scale = lax.rsqrt(squares / D + epsilon)[:, None]
    return (jax.nn.silu(row_scale * gate_acc) * (row_scale * up_acc)).astype(jnp.bfloat16)


def down_sum(hidden, w_down):
    return lax.psum_scatter(
        jnp.dot(hidden, w_down, preferred_element_type=jnp.float32),
        ("kv", "tp"),
        scatter_dimension=1,
        tiled=True,
    )


def per_device_plain(
    tokens,
    past_state,
    pre_gain,
    pre_gate,
    pre_up,
    pre_down,
    mix_gain,
    query_weight,
    forget_weight,
    value_weight,
    output_gate_weight,
    forget_floor,
    head_gain,
    proj_out,
    post_gain,
    post_gate,
    post_up,
    post_down,
):
    whole_rows = lax.all_gather(tokens, ("kv", "tp"), axis=1, tiled=True)
    whole_float = whole_rows.astype(jnp.float32)
    row_scale = lax.rsqrt(jnp.mean(whole_float * whole_float, axis=1, keepdims=True) + epsilon)
    normed = (whole_float * pre_gain).astype(jnp.bfloat16)
    gate_pre = row_scale * jnp.dot(normed, pre_gate, preferred_element_type=jnp.float32)
    up_pre = row_scale * jnp.dot(normed, pre_up, preferred_element_type=jnp.float32)
    hidden = (jax.nn.silu(gate_pre) * up_pre).astype(jnp.bfloat16)
    kv_sums = lax.psum_scatter(
        jnp.dot(hidden, pre_down, preferred_element_type=jnp.float32).astype(jnp.bfloat16),
        "kv",
        scatter_dimension=1,
        tiled=True,
    )
    block_sum = lax.psum(kv_sums, "tp").astype(jnp.float32)
    block_width = block_sum.shape[1]
    block_old = lax.dynamic_slice_in_dim(
        whole_rows, lax.axis_index("kv") * block_width, block_width, 1
    )
    block_rows = (block_old.astype(jnp.float32) + 0.5 * block_sum).astype(jnp.bfloat16)
    own_width = block_width // lax.axis_size("tp")
    after_first = lax.dynamic_slice_in_dim(
        block_rows, lax.axis_index("tp") * own_width, own_width, 1
    )
    block_width = block_rows.shape[1]
    block_float = block_rows.astype(jnp.float32)
    block_gain = lax.dynamic_slice_in_dim(
        mix_gain, lax.axis_index("kv") * block_width, block_width, 0
    )
    squares = lax.psum(jnp.sum(block_float * block_float, axis=1), "kv")
    normed = (block_float * block_gain).astype(jnp.bfloat16)
    own_rows = past_state.shape[0]
    weight_list = (query_weight, forget_weight, value_weight, output_gate_weight)
    projected = lax.psum_scatter(
        jnp.concatenate(
            [
                jnp.dot(normed, weight_part, preferred_element_type=jnp.float32)
                for weight_part in weight_list
            ],
            axis=1,
        ).astype(jnp.bfloat16),
        "kv",
        scatter_dimension=0,
        tiled=True,
    ).astype(jnp.float32)
    own_squares = lax.dynamic_slice_in_dim(squares, lax.axis_index("kv") * own_rows, own_rows, 0)
    projected = projected * lax.rsqrt(own_squares / D + epsilon)[:, None]
    pre_query, pre_forget, pre_value, pre_gate_out = jnp.split(projected, 4, axis=1)
    local_heads = past_state.shape[1]
    head_width = past_state.shape[2]
    head_shape = (own_rows, local_heads, head_width)
    floors = forget_floor.reshape(local_heads, head_width)
    forget_heads = pre_forget.reshape(head_shape)
    forget = floors + (1.0 - floors) * jax.nn.sigmoid(forget_heads)
    written = (1.0 - floors) * jax.nn.sigmoid(-forget_heads)
    query_act = jax.nn.silu(pre_query.reshape(head_shape))
    value_act = pre_value.reshape(head_shape)
    new_state = (
        forget[:, :, :, None] * past_state + written[:, :, :, None] * value_act[:, :, None, :]
    )
    readout = jnp.einsum("bhkv,bhk->bhv", new_state, query_act, precision=lax.Precision.HIGHEST)
    readout = (
        readout
        * lax.rsqrt(jnp.mean(readout * readout, axis=2, keepdims=True) + epsilon)
        * head_gain
    )
    mixed_in = (
        readout.reshape(own_rows, local_heads * head_width) * jax.nn.silu(pre_gate_out)
    ).astype(jnp.bfloat16)
    partials = jnp.dot(
        lax.all_gather(mixed_in, "kv", axis=0, tiled=True),
        proj_out,
        preferred_element_type=jnp.float32,
    ).astype(jnp.bfloat16)
    mixed_sum = lax.psum_scatter(partials, "tp", scatter_dimension=1, tiled=True).astype(
        jnp.float32
    )
    second = (after_first.astype(jnp.float32) + mixed_sum).astype(jnp.bfloat16)
    hidden_two = half_inputs(second, post_gain, post_gate, post_up)
    result = (second.astype(jnp.float32) + 0.5 * down_sum(hidden_two, post_down)).astype(
        jnp.bfloat16
    )
    return (result, new_state)


LANES = 128
LAST = (((1,), (1,)), ((), ()))
CORES = 2
F32, BF16 = jnp.float32, jnp.bfloat16
MESH = pl.DeviceIdType.MESH


class Grid:
    def __init__(self, n_kv, n_tp):
        self.nk, self.nt, self.nx = n_kv, n_tp, n_tp // CORES
        self.kv, self.tp = lax.axis_index("kv"), lax.axis_index("tp")
        self.x, self.c = self.tp // CORES, self.tp % CORES
        self.oc = 1 - self.c

    def k(self, step):
        return lax.rem(self.kv + step, self.nk)

    def xi(self, step):
        return lax.rem(self.x + step, self.nx)

    def t(self, step):
        return lax.rem(self.tp + step, self.nt)

    def block(self, k, x, c):
        return k * self.nt + x * CORES + c


def remote(src, dst, send, recv, k, t):
    return pltpu.make_async_remote_copy(
        src_ref=src, dst_ref=dst, send_sem=send, recv_sem=recv,
        device_id={"kv": k, "tp": t}, device_id_type=MESH,
    )


def barrier(g):
    sem = pltpu.get_barrier_semaphore()
    for step in range(1, g.nk):
        pl.semaphore_signal(sem, inc=1, device_id={"kv": g.k(step), "tp": g.tp}, device_id_type=MESH)
    for step in range(1, g.nt):
        pl.semaphore_signal(sem, inc=1, device_id={"kv": g.kv, "tp": g.t(step)}, device_id_type=MESH)
    pl.semaphore_wait(sem, g.nk - 1 + g.nt - 1)


def cols(ref, block, width=LANES):
    return ref.at[:, pl.ds(pl.multiple_of(block * width, LANES), width)]


def gather_all(g, own_ref, full, send_k, send_x, send_c, recv):
    started = []

    def put(src, block, sem, k, t):
        copy = remote(src, cols(full, block), sem, recv.at[block], k, t)
        copy.start()
        started.append(copy)

    def arrived(block):
        remote(own_ref, cols(full, block), send_k.at[0], recv.at[block], g.kv, g.tp).wait_recv()

    mine = g.block(g.kv, g.x, g.c)
    for step in range(1, g.nk):
        put(own_ref, mine, send_k.at[step], g.k(step), g.tp)
    for dx in range(1, g.nx):
        put(own_ref, mine, send_x.at[0, dx], g.kv, g.xi(dx) * CORES + g.c)
    put(own_ref, mine, send_c.at[0, 0], g.kv, g.x * CORES + g.oc)
    full[:, pl.ds(pl.multiple_of(mine * LANES, LANES), LANES)] = own_ref[...]

    def cross(step):
        k = g.k(g.nk - step)
        for dx in range(1, g.nx):
            block = g.block(k, g.xi(dx), g.c)
            arrived(block)
            put(cols(full, block), block, send_c.at[step, dx], g.kv, g.x * CORES + g.oc)

    for step in range(1, g.nk):
        block = g.block(g.k(g.nk - step), g.x, g.c)
        arrived(block)
        for dx in range(1, g.nx):
            put(cols(full, block), block, send_x.at[step, dx], g.kv, g.xi(dx) * CORES + g.c)
        put(cols(full, block), block, send_c.at[step, 0], g.kv, g.x * CORES + g.oc)
        cross(step - 1)
    cross(g.nk - 1)
    for step in range(g.nk):
        for dx in range(g.nx):
            arrived(g.block(g.k(g.nk - step), g.xi(dx), g.oc))
    for copy in started:
        copy.wait_send()


def hidden_units(full, gain_ref, wg, wu, acc_g, acc_u, hidden, width):
    rows, depth = full.shape
    acc_g[...] = jnp.zeros_like(acc_g)
    acc_u[...] = jnp.zeros_like(acc_u)

    def body(i, squares):
        at = pl.ds(pl.multiple_of(i * width, LANES), width)
        x = full[:, at].astype(F32)
        u = (x * gain_ref[:, at]).astype(BF16)
        acc_g[...] += lax.dot_general(u, wg[:, at], LAST, preferred_element_type=F32)
        acc_u[...] += lax.dot_general(u, wu[:, at], LAST, preferred_element_type=F32)
        return squares + jnp.sum(x * x, axis=1, keepdims=True)

    squares = lax.fori_loop(0, depth // width, body, jnp.zeros((rows, 1), F32))
    scale = lax.rsqrt(squares / depth + epsilon)
    hidden[...] = (jax.nn.silu(scale * acc_g[...]) * (scale * acc_u[...])).astype(BF16)


def down_scatter(g, hidden, wd, part, sib, out_x, in_x, keep, out_k, in_k, sa, ra, sb, rb, sc, rc):
    width = g.nt * LANES
    last = g.nk - 1

    def kof(i):
        return g.k(i + 1)

    def copy_a(i, xx):
        src = cols(part, g.block(kof(i), xx, g.oc))
        return remote(src, sib.at[i, xx], sa.at[i, xx], ra.at[i, xx], g.kv, g.x * CORES + g.oc)

    def copy_b(i, dx):
        return remote(out_x.at[i, dx - 1], in_x.at[i, dx - 1], sb.at[i, dx - 1], rb.at[i, dx - 1], g.kv, g.xi(dx) * CORES + g.c)

    def copy_c(i):
        return remote(out_k.at[i], in_k.at[i], sc.at[i], rc.at[i], kof(i), g.tp)

    def stage_a(i):
        at = pl.ds(pl.multiple_of(kof(i) * width, LANES), width)
        part[:, at] = jnp.dot(hidden[...], wd[:, at], preferred_element_type=F32).astype(BF16)
        for xx in range(g.nx):
            copy_a(i, xx).start()

    def pair_sum(i, xx):
        at = pl.ds(pl.multiple_of(g.block(kof(i), xx, g.c) * LANES, LANES), LANES)
        return part[:, at].astype(F32) + sib[i, xx].astype(F32)

    def stage_b(i):
        for xx in range(g.nx):
            copy_a(i, xx).wait_recv()
        for dx in range(1, g.nx):
            out_x[i, dx - 1] = pair_sum(i, g.xi(dx)).astype(BF16)
            copy_b(i, dx).start()
        keep[i % 2] = pair_sum(i, g.x)

    def stage_c(i):
        for dx in range(1, g.nx):
            copy_b(i, dx).wait_recv()
        total = keep[i % 2]
        for dx in range(1, g.nx):
            total = total + in_x[i, dx - 1].astype(F32)
        return total

    def send_c(i):
        out_k[i] = stage_c(i).astype(BF16)
        copy_c(i).start()

    stage_a(0)
    stage_a(1)
    stage_b(0)

    def body(i, carry):
        stage_a(i)
        send_c(i - 2)
        stage_b(i - 1)
        return carry

    lax.fori_loop(2, g.nk, body, 0)
    send_c(last - 1)
    stage_b(last)
    total = stage_c(last)
    for i in range(last):
        copy_c(i).wait_recv()
        total = total + in_k[i].astype(F32)
    for i in range(g.nk):
        for xx in range(g.nx):
            copy_a(i, xx).wait_send()
        for dx in range(1, g.nx):
            copy_b(i, dx).wait_send()
        if i < last:
            copy_c(i).wait_send()
    return total


def ff_scratch(nk, nt, rows, depth, units):
    nx = nt // CORES
    dma = pltpu.SemaphoreType.DMA
    weights = [
        pltpu.VMEM((units, depth), BF16),
        pltpu.VMEM((units, depth), BF16),
        pltpu.VMEM((units, depth), BF16),
        dma((3,)),
    ]
    gather = [
        pltpu.VMEM((rows, depth), BF16),
        dma((nk,)),
        dma((nk, nx)),
        dma((nk, nx)),
        dma((nk * nt,)),
    ]
    mid = [pltpu.VMEM((rows, units), F32), pltpu.VMEM((rows, units), F32), pltpu.VMEM((rows, units), BF16)]
    scatter = [
        pltpu.VMEM((rows, depth), BF16),
        pltpu.VMEM((nk, nx, rows, LANES), BF16),
        pltpu.VMEM((nk, nx - 1, rows, LANES), BF16),
        pltpu.VMEM((nk, nx - 1, rows, LANES), BF16),
        pltpu.VMEM((2, rows, LANES), F32),
        pltpu.VMEM((nk - 1, rows, LANES), BF16),
        pltpu.VMEM((nk - 1, rows, LANES), BF16),
        dma((nk, nx)),
        dma((nk, nx)),
        dma((nk, nx - 1)),
        dma((nk, nx - 1)),
        dma((nk - 1,)),
        dma((nk - 1,)),
    ]
    return weights + gather + mid + scatter


N_FF = 4 + 5 + 3 + 13


def load_weights(hbm, vmem, sem):
    copies = [pltpu.make_async_copy(a, b, sem.at[i]) for i, (a, b) in enumerate(zip(hbm, vmem))]
    for copy in copies:
        copy.start()
    return copies


def run_ff(g, own_ref, gain_ref, loads, ff):
    wg, wu, wd, _ = ff[:4]
    full, send_k, send_x, send_c, recv = ff[4:9]
    acc_g, acc_u, hidden = ff[9:12]
    gather_all(g, own_ref, full, send_k, send_x, send_c, recv)
    loads[0].wait()
    loads[1].wait()
    hidden_units(full, gain_ref, wg, wu, acc_g, acc_u, hidden, full.shape[1] // g.nk)
    loads[2].wait()
    total = down_scatter(g, hidden, wd, *ff[12:])
    return own_ref[...].astype(F32) + 0.5 * total


def first_kernel(nk, nt, tok, gain, mgain, wg_h, wu_h, wd_h, q_h, f_h, v_h, o_h, first, projected, *scratch):
    g = Grid(nk, nt)
    ff, rest = scratch[:N_FF], scratch[N_FF:]
    mixw, mix_sem, block, bsend, brecv, normed, proj, mate_got, sums, got, sq, sq_got, msend, mrecv, psend, precv, qsend, qrecv = rest
    loads = load_weights((wg_h, wu_h, wd_h), ff[:3], ff[3])
    mix_loads = load_weights((q_h, f_h, v_h, o_h), [mixw.at[i] for i in range(4)], mix_sem)
    barrier(g)
    first[...] = run_ff(g, tok, gain, loads, ff).astype(BF16)

    copies = []
    for step in range(1, nt):
        copy = remote(first, cols(block, g.tp), bsend.at[step - 1], brecv.at[step - 1], g.kv, g.t(step))
        copy.start()
        copies.append(copy)
    block[:, pl.ds(pl.multiple_of(g.tp * LANES, LANES), LANES)] = first[...]
    for step in range(1, nt):
        src = g.t(nt - step)
        remote(first, cols(block, src), bsend.at[step - 1], brecv.at[step - 1], g.kv, src).wait_recv()
    width = block.shape[1]
    x = block[...].astype(F32)
    normed[...] = (x * mgain[:, pl.ds(pl.multiple_of(g.kv * width, LANES), width)]).astype(BF16)
    sq[...] = jnp.broadcast_to(jnp.sum(x * x, axis=1, keepdims=True), sq.shape)
    own_rows, inner = projected.shape[0], projected.shape[1] // 4

    def rows_of(k):
        return pl.ds(pl.multiple_of(k * own_rows, own_rows), own_rows)

    def q_copy(step):
        return remote(sq.at[rows_of(g.k(step))], sq_got.at[step - 1], qsend.at[step - 1], qrecv.at[step - 1], g.k(step), g.tp)

    nz, z, y = nk // 2, g.kv // 2, g.kv % 2

    def zi(dz):
        return lax.rem(z + dz, nz)

    def m_copy(i, dz):
        src = proj.at[i, zi(dz) * 2 + 1 - y]
        return remote(src, mate_got.at[i, dz], msend.at[i, dz], mrecv.at[i, dz], 2 * z + 1 - y, g.tp)

    def p_copy(i, dz):
        at = dz - 1
        return remote(sums.at[i, at], got.at[i, at], psend.at[i, at], precv.at[i, at], zi(dz) * 2 + y, g.tp)

    def mate_sum(i, dz):
        m_copy(i, dz).wait_recv()
        return proj[i, zi(dz) * 2 + y].astype(F32) + mate_got[i, dz].astype(F32)

    def forward(i):
        for dz in range(1, nz):
            sums[i, dz - 1] = mate_sum(i, dz).astype(BF16)
            p_copy(i, dz).start()

    for step in range(1, nk):
        q_copy(step).start()
    for i in range(4):
        mix_loads[i].wait()
        out = jnp.dot(normed[...], mixw[i], preferred_element_type=F32).astype(BF16)
        proj[i] = out.reshape(nk, own_rows, inner)
        for dz in range(1, nz + 1):
            m_copy(i, dz % nz).start()
        if i:
            forward(i - 1)
    forward(3)
    squares = sq[rows_of(g.kv), :]
    for step in range(1, nk):
        q_copy(step).wait_recv()
        squares = squares + sq_got[step - 1]
    scale = lax.rsqrt(squares[:, :1] / mgain.shape[1] + epsilon)
    for i in range(4):
        total = mate_sum(i, 0)
        for dz in range(1, nz):
            p_copy(i, dz).wait_recv()
            total = total + got[i, dz - 1].astype(F32)
        projected[:, i * inner : (i + 1) * inner] = total * scale
    for copy in copies:
        copy.wait_send()
    for step in range(1, nk):
        q_copy(step).wait_send()
    for i in range(4):
        for dz in range(nz):
            m_copy(i, dz).wait_send()
        for dz in range(1, nz):
            p_copy(i, dz).wait_send()


def recurrence_kernel(projected, past, floor, head_gain, new, mixed):
    rows, heads, width = past.shape[:3]
    inner = heads * width
    for h in range(heads):
        def part(i):
            return projected[:, i * inner + h * width : i * inner + (h + 1) * width]

        at = slice(h * width, (h + 1) * width)
        base = floor[:, at]
        forget = (base + (1.0 - base) * jax.nn.sigmoid(part(1))).T
        written = ((1.0 - base) * jax.nn.sigmoid(-part(1))).T
        query = jax.nn.silu(part(0)).T
        value = part(2)
        outs = []
        for n in range(rows):
            col = slice(n, n + 1)
            state = forget[:, col] * past[n, h] + written[:, col] * value[col]
            new[n, h] = state
            outs.append(jnp.sum(state * query[:, col], axis=0, keepdims=True))
        read = jnp.concatenate(outs, axis=0)
        read = read * lax.rsqrt(jnp.mean(read * read, axis=1, keepdims=True) + epsilon) * head_gain[...]
        mixed[:, at] = (read * jax.nn.silu(part(3))).astype(BF16)


def recurrence(projected, past_state, forget_floor, head_gain):
    rows, heads, width = past_state.shape[:3]
    inner, step = heads * width, 8
    state_spec = pl.BlockSpec((step, heads, width, width), lambda i: (i, 0, 0, 0))
    return pl.pallas_call(
        recurrence_kernel,
        grid=(rows // step,),
        out_shape=(
            jax.ShapeDtypeStruct(past_state.shape, F32),
            jax.ShapeDtypeStruct((rows, inner), BF16),
        ),
        in_specs=[
            pl.BlockSpec((step, 4 * inner), lambda i: (i, 0)),
            state_spec,
            pl.BlockSpec((1, inner), lambda i: (0, 0)),
            pl.BlockSpec((1, width), lambda i: (0, 0)),
        ],
        out_specs=(state_spec, pl.BlockSpec((step, inner), lambda i: (i, 0))),
        compiler_params=pltpu.CompilerParams(vmem_limit_bytes=32 * 1024 * 1024),
    )(projected, past_state, forget_floor[None], head_gain[None])


def second_kernel(nk, nt, y, first, gain, po_h, wg_h, wu_h, wd_h, result, *scratch):
    g = Grid(nk, nt)
    ff, rest = scratch[:N_FF], scratch[N_FF:]
    po, po_sem, yfull, ysend, yrecv, part, got, tsend, trecv, second = rest
    po_load = load_weights((po_h,), (po,), po_sem)
    loads = load_weights((wg_h, wu_h, wd_h), ff[:3], ff[3])
    barrier(g)
    own_rows = y.shape[0]

    def rows_of(k):
        return pl.ds(pl.multiple_of(k * own_rows, own_rows), own_rows)

    def y_copy(step, k, src):
        return remote(y, yfull.at[rows_of(src)], ysend.at[step - 1], yrecv.at[step - 1], k, g.tp)

    for step in range(1, nk):
        y_copy(step, g.k(step), g.kv).start()
    yfull[rows_of(g.kv), :] = y[...]
    for step in range(1, nk):
        y_copy(step, g.k(step), g.k(nk - step)).wait_recv()
    po_load[0].wait()
    part[...] = jnp.dot(yfull[...], po[...], preferred_element_type=F32).astype(BF16)

    def t_copy(step):
        return remote(cols(part, g.t(step)), got.at[step - 1], tsend.at[step - 1], trecv.at[step - 1], g.kv, g.t(step))

    for step in range(1, nt):
        t_copy(step).start()
    total = part[:, pl.ds(pl.multiple_of(g.tp * LANES, LANES), LANES)].astype(F32)
    for step in range(1, nt):
        t_copy(step).wait_recv()
        total = total + got[step - 1].astype(F32)
    second[...] = (first[...].astype(F32) + total).astype(BF16)
    result[...] = run_ff(g, second, gain, loads, ff).astype(BF16)
    for step in range(1, nk):
        y_copy(step, g.k(step), g.kv).wait_send()
    for step in range(1, nt):
        t_copy(step).wait_send()


def call(kernel, ident, outs, n_vmem, n_any, scratch, args):
    vmem, any_space = pl.BlockSpec(memory_space=pltpu.VMEM), pl.BlockSpec(memory_space=pl.ANY)
    return pl.pallas_call(
        kernel,
        out_shape=outs,
        in_specs=[vmem] * n_vmem + [any_space] * n_any,
        out_specs=jax.tree.map(lambda _: vmem, outs),
        scratch_shapes=scratch,
        compiler_params=pltpu.CompilerParams(
            collective_id=ident, has_side_effects=True, vmem_limit_bytes=56 * 1024 * 1024
        ),
    )(*args)


def per_device(
    tokens, past_state, pre_gain, pre_gate, pre_up, pre_down, mix_gain,
    query_weight, forget_weight, value_weight, output_gate_weight,
    forget_floor, head_gain, proj_out, post_gain, post_gate, post_up, post_down,
):
    nk, nt = lax.axis_size("kv"), lax.axis_size("tp")
    rows, depth, units = tokens.shape[0], pre_gate.shape[0], pre_gate.shape[1]
    own_rows, local_heads, head_width = past_state.shape[:3]
    inner = local_heads * head_width
    width = query_weight.shape[0]
    dma = pltpu.SemaphoreType.DMA
    base = ff_scratch(nk, nt, rows, depth, units)
    first, projected = call(
        functools.partial(first_kernel, nk, nt),
        0,
        (jax.ShapeDtypeStruct(tokens.shape, BF16), jax.ShapeDtypeStruct((own_rows, 4 * inner), F32)),
        3,
        7,
        base
        + [
            pltpu.VMEM((4, width, inner), BF16),
            dma((4,)),
            pltpu.VMEM((rows, width), BF16),
            dma((nt - 1,)),
            dma((nt - 1,)),
            pltpu.VMEM((rows, width), BF16),
            pltpu.VMEM((4, nk, own_rows, inner), BF16),
            pltpu.VMEM((4, nk // 2, own_rows, inner), BF16),
            pltpu.VMEM((4, nk // 2 - 1, own_rows, inner), BF16),
            pltpu.VMEM((4, nk // 2 - 1, own_rows, inner), BF16),
            pltpu.VMEM((rows, LANES), F32),
            pltpu.VMEM((nk - 1, own_rows, LANES), F32),
            dma((4, nk // 2)),
            dma((4, nk // 2)),
            dma((4, nk // 2 - 1)),
            dma((4, nk // 2 - 1)),
            dma((nk - 1,)),
            dma((nk - 1,)),
        ],
        (
            tokens, pre_gain[None], mix_gain[None], pre_gate.T, pre_up.T, pre_down,
            query_weight, forget_weight, value_weight, output_gate_weight,
        ),
    )
    new_state, mixed_in = recurrence(projected, past_state, forget_floor, head_gain)
    result = call(
        functools.partial(second_kernel, nk, nt),
        1,
        jax.ShapeDtypeStruct(tokens.shape, BF16),
        3,
        4,
        base
        + [
            pltpu.VMEM(proj_out.shape, BF16),
            dma((1,)),
            pltpu.VMEM((rows, inner), BF16),
            dma((nk - 1,)),
            dma((nk - 1,)),
            pltpu.VMEM((rows, width), BF16),
            pltpu.VMEM((nt - 1, rows, LANES), BF16),
            dma((nt - 1,)),
            dma((nt - 1,)),
            pltpu.VMEM((rows, LANES), BF16),
        ],
        (mixed_in, first, post_gain[None], proj_out, post_gate.T, post_up.T, post_down),
    )
    return (result, new_state)


def solution(mesh):
    placed = (
        P(None, ("kv", "tp")),
        P("kv", "tp", None, None),
        P(),
        P(None, ("kv", "tp")),
        P(None, ("kv", "tp")),
        P(("kv", "tp"), None),
        P(),
        P("kv", "tp"),
        P("kv", "tp"),
        P("kv", "tp"),
        P("kv", "tp"),
        P("tp"),
        P(),
        P("tp", "kv"),
        P(),
        P(None, ("kv", "tp")),
        P(None, ("kv", "tp")),
        P(("kv", "tp"), None),
    )
    blocks_fit = D == mesh.shape["kv"] * mesh.shape["tp"] * LANES and mesh.shape["tp"] >= 2 * CORES
    return jax.shard_map(
        per_device if blocks_fit else per_device_plain,
        mesh=mesh,
        in_specs=placed,
        out_specs=(P(None, ("kv", "tp")), P("kv", "tp", None, None)),
        check_vma=False,
    )
```

profile of v0, /device:TPU:0, one launch (start us, length us, event | category | flops | bytes accessed | tf_op | source)
XLA Modules:
  0.0 172.9 jit_solution(11028492370589761908)
XLA Ops:
  0.6 0.0 copy-start.3
  0.6 0.0 copy-start.4
  0.7 86.0 %shard_map.185 = (bf16[256,128]{1,0:T(8,128)(2,1)}, f32[32,2048]{1,0:T(8,128)}) custom-call(bf16[256,128]{1,0:T(8,128)(2,1)} %tok.1, f32[1,4096]{1,0:T(1,128)} %bitcast.15, f32[1,4096]{1,0:T(1,128)} %bitcast.16, bf16[352,4096]{1,0:T(8,128)(2,1)} %bitcast.11, bf16[352,4096]{1,0:T(8,128)(2,1)} %bitcast.12, bf16[352,4096]{1,0:T(8,128)(2,1)} %wd_h.2, ...), custom_call_target="tpu_custom_call" | custom-call | tf_op jit(solution)/shard_map/pallas_call | solution.py:550
  86.7 0.0 copy-done.3
  86.7 0.0 copy-done.4
  86.7 0.0 copy-start
  86.7 3.4 %copy-done = f32[32,4,128,128]{3,2,1,0:T(8,128)S(1)} copy-done((f32[32,4,128,128]{3,2,1,0:T(8,128)S(1)}, f32[32,4,128,128]{3,2,1,0:T(8,128)}, u32[]{:S(2)}) %copy-start) | copy-done | bytes 8388632
  90.1 0.0 copy-start.1
  90.1 0.9 copy-done.1
  91.0 10.7 %shard_map.186 = (f32[32,4,128,128]{3,2,1,0:T(8,128)}, bf16[32,512]{1,0:T(8,128)(2,1)S(1)}) custom-call(f32[32,2048]{1,0:T(8,128)S(1)} %copy-done.1, f32[32,4,128,128]{3,2,1,0:T(8,128)S(1)} %copy-done, f32[1,512]{1,0:T(1,128)S(1)} %bitcast.9, f32[1,128]{1,0:T(1,128)S(1)} %bitcast.10), custom_call_target="tpu_custom_call" | custom-call | tf_op jit(solution)/shard_map/pallas_call | solution.py:490
  101.7 0.0 copy-start.2
  101.7 0.6 copy-done.2
  102.3 69.1 %shard_map.187 = bf16[256,128]{1,0:T(8,128)(2,1)} custom-call(bf16[32,512]{1,0:T(8,128)(2,1)} %copy-done.2, bf16[256,128]{1,0:T(8,128)(2,1)} %get-tuple-element.8.first, f32[1,4096]{1,0:T(1,128)} %bitcast.17, bf16[512,512]{1,0:T(8,128)(2,1)} %po_h.1, bf16[352,4096]{1,0:T(8,128)(2,1)} %bitcast.13, bf16[352,4096]{1,0:T(8,128)(2,1)} %bitcast.14, ...), custom_call_target="tpu_custom_call" | custom-call | tf_op jit(solution)/shard_map/pallas_call | solution.py:550
  171.4 1.5 copy.21
Async XLA Ops:
  0.6 86.0 %copy-start.3 = (f32[512]{0:T(512)S(1)}, f32[512]{0:T(512)}, u32[]{:S(2)}) copy-start(f32[512]{0:T(512)} %param.29) | copy-start | bytes 6148
  0.6 86.0 %copy-start.4 = (f32[128]{0:T(128)S(1)}, f32[128]{0:T(128)}, u32[]{:S(2)}) copy-start(f32[128]{0:T(128)} %param.30) | copy-start | bytes 1540
  86.7 3.4 %copy-start = (f32[32,4,128,128]{3,2,1,0:T(8,128)S(1)}, f32[32,4,128,128]{3,2,1,0:T(8,128)}, u32[]{:S(2)}) copy-start(f32[32,4,128,128]{3,2,1,0:T(8,128)} %past.1) | copy-start | bytes 25165828
  90.1 0.9 copy-start.1
  101.7 0.6 copy-start.2
where the time goes:
time: 174 us; the launch traced here: 173 us
  Pallas kernels  166 us (95%)
  local copies, waits for them, and re-layouts  6.42 us (4%)
    pallas_call x2, Pallas kernels, call(): pl.pallas_call(kernel, out_shape=outs, in_specs=[vmem] * n_vmem + [any_sp...  155 us
    pallas_call x1, Pallas kernels, recurrence(): pl.pallas_call(recurrence_kernel, grid=(rows // step,), out_shape=(jax.Sh...  10.7 us
    unnamed x11, local copies, waits for them, and re-layouts  6.42 us

commit v1 on v0

--- a/solution.py
+++ b/solution.py
@@ -138,29 +138,41 @@
 
 LANES = 128
 LAST = (((1,), (1,)), ((), ()))
-CORES = 2
+FIRST = (((0,), (0,)), ((), ()))
+CORES, LINE, SIDE = 2, 4, 2
+PLANE = SIDE * SIDE
 F32, BF16 = jnp.float32, jnp.bfloat16
 MESH = pl.DeviceIdType.MESH
 
 
 class Grid:
     def __init__(self, n_kv, n_tp):
-        self.nk, self.nt, self.nx = n_kv, n_tp, n_tp // CORES
+        self.nk, self.nt = n_kv, n_tp
         self.kv, self.tp = lax.axis_index("kv"), lax.axis_index("tp")
+        self.z, self.y = self.kv // SIDE, self.kv % SIDE
         self.x, self.c = self.tp // CORES, self.tp % CORES
         self.oc = 1 - self.c
+        y, x, c = self.y, self.x, self.c
+        self.own = (y, x)
+        self.a = (y + c * (1 - 2 * y), x + (1 - c) * (1 - 2 * x))
+        self.b = (y + (1 - c) * (1 - 2 * y), x + c * (1 - 2 * x))
+        self.diag = (1 - y, 1 - x)
+        self.z1 = self.z + 1 - 2 * (self.z % 2)
+        self.z3 = LINE - 1 - self.z
+        self.z2 = LINE - 1 - self.z1
+        self.mid = (self.z == 1) | (self.z == 2)
 
     def k(self, step):
         return lax.rem(self.kv + step, self.nk)
 
-    def xi(self, step):
-        return lax.rem(self.x + step, self.nx)
-
     def t(self, step):
         return lax.rem(self.tp + step, self.nt)
 
-    def block(self, k, x, c):
-        return k * self.nt + x * CORES + c
+    def block(self, z, yx, c):
+        return (z * SIDE + yx[0]) * self.nt + yx[1] * CORES + c
+
+    def at(self, z, yx, c):
+        return z * SIDE + yx[0], yx[1] * CORES + c
 
 
 def remote(src, dst, send, recv, k, t):
@@ -168,6 +180,25 @@
         src_ref=src, dst_ref=dst, send_sem=send, recv_sem=recv,
         device_id={"kv": k, "tp": t}, device_id_type=MESH,
     )
+
+
+class Sends:
+    def __init__(self):
+        self.started = []
+
+    def start(self, copy, when=None):
+        if when is None:
+            copy.start()
+        else:
+            pl.when(when)(copy.start)
+        self.started.append((copy, when))
+
+    def finish(self):
+        for copy, when in self.started:
+            if when is None:
+                copy.wait_send()
+            else:
+                pl.when(when)(copy.wait_send)
 
 
 def barrier(g):
@@ -179,179 +210,52 @@
     pl.semaphore_wait(sem, g.nk - 1 + g.nt - 1)
 
 
+def lanes(index, width=LANES):
+    return pl.ds(pl.multiple_of(index * width, LANES), width)
+
+
 def cols(ref, block, width=LANES):
-    return ref.at[:, pl.ds(pl.multiple_of(block * width, LANES), width)]
-
-
-def gather_all(g, own_ref, full, send_k, send_x, send_c, recv):
-    started = []
-
-    def put(src, block, sem, k, t):
-        copy = remote(src, cols(full, block), sem, recv.at[block], k, t)
-        copy.start()
-        started.append(copy)
-
-    def arrived(block):
-        remote(own_ref, cols(full, block), send_k.at[0], recv.at[block], g.kv, g.tp).wait_recv()
-
-    mine = g.block(g.kv, g.x, g.c)
-    for step in range(1, g.nk):
-        put(own_ref, mine, send_k.at[step], g.k(step), g.tp)
-    for dx in range(1, g.nx):
-        put(own_ref, mine, send_x.at[0, dx], g.kv, g.xi(dx) * CORES + g.c)
-    put(own_ref, mine, send_c.at[0, 0], g.kv, g.x * CORES + g.oc)
-    full[:, pl.ds(pl.multiple_of(mine * LANES, LANES), LANES)] = own_ref[...]
-
-    def cross(step):
-        k = g.k(g.nk - step)
-        for dx in range(1, g.nx):
-            block = g.block(k, g.xi(dx), g.c)
-            arrived(block)
-            put(cols(full, block), block, send_c.at[step, dx], g.kv, g.x * CORES + g.oc)
-
-    for step in range(1, g.nk):
-        block = g.block(g.k(g.nk - step), g.x, g.c)
-        arrived(block)
-        for dx in range(1, g.nx):
-            put(cols(full, block), block, send_x.at[step, dx], g.kv, g.xi(dx) * CORES + g.c)
-        put(cols(full, block), block, send_c.at[step, 0], g.kv, g.x * CORES + g.oc)
-        cross(step - 1)
-    cross(g.nk - 1)
-    for step in range(g.nk):
-        for dx in range(g.nx):
-            arrived(g.block(g.k(g.nk - step), g.xi(dx), g.oc))
-    for copy in started:
-        copy.wait_send()
-
-
-def hidden_units(full, gain_ref, wg, wu, acc_g, acc_u, hidden, width):
-    rows, depth = full.shape
-    acc_g[...] = jnp.zeros_like(acc_g)
-    acc_u[...] = jnp.zeros_like(acc_u)
-
-    def body(i, squares):
-        at = pl.ds(pl.multiple_of(i * width, LANES), width)
-        x = full[:, at].astype(F32)
-        u = (x * gain_ref[:, at]).astype(BF16)
-        acc_g[...] += lax.dot_general(u, wg[:, at], LAST, preferred_element_type=F32)
-        acc_u[...] += lax.dot_general(u, wu[:, at], LAST, preferred_element_type=F32)
-        return squares + jnp.sum(x * x, axis=1, keepdims=True)
-
-    squares = lax.fori_loop(0, depth // width, body, jnp.zeros((rows, 1), F32))
-    scale = lax.rsqrt(squares / depth + epsilon)
-    hidden[...] = (jax.nn.silu(scale * acc_g[...]) * (scale * acc_u[...])).astype(BF16)
-
-
-def down_scatter(g, hidden, wd, part, sib, out_x, in_x, keep, out_k, in_k, sa, ra, sb, rb, sc, rc):
-    width = g.nt * LANES
-    last = g.nk - 1
-
-    def kof(i):
-        return g.k(i + 1)
-
-    def copy_a(i, xx):
-        src = cols(part, g.block(kof(i), xx, g.oc))
-        return remote(src, sib.at[i, xx], sa.at[i, xx], ra.at[i, xx], g.kv, g.x * CORES + g.oc)
-
-    def copy_b(i, dx):
-        return remote(out_x.at[i, dx - 1], in_x.at[i, dx - 1], sb.at[i, dx - 1], rb.at[i, dx - 1], g.kv, g.xi(dx) * CORES + g.c)
-
-    def copy_c(i):
-        return remote(out_k.at[i], in_k.at[i], sc.at[i], rc.at[i], kof(i), g.tp)
-
-    def stage_a(i):
-        at = pl.ds(pl.multiple_of(kof(i) * width, LANES), width)
-        part[:, at] = jnp.dot(hidden[...], wd[:, at], preferred_element_type=F32).astype(BF16)
-        for xx in range(g.nx):
-            copy_a(i, xx).start()
-
-    def pair_sum(i, xx):
-        at = pl.ds(pl.multiple_of(g.block(kof(i), xx, g.c) * LANES, LANES), LANES)
-        return part[:, at].astype(F32) + sib[i, xx].astype(F32)
-
-    def stage_b(i):
-        for xx in range(g.nx):
-            copy_a(i, xx).wait_recv()
-        for dx in range(1, g.nx):
-            out_x[i, dx - 1] = pair_sum(i, g.xi(dx)).astype(BF16)
-            copy_b(i, dx).start()
-        keep[i % 2] = pair_sum(i, g.x)
-
-    def stage_c(i):
-        for dx in range(1, g.nx):
-            copy_b(i, dx).wait_recv()
-        total = keep[i % 2]
-        for dx in range(1, g.nx):
-            total = total + in_x[i, dx - 1].astype(F32)
-        return total
-
-    def send_c(i):
-        out_k[i] = stage_c(i).astype(BF16)
-        copy_c(i).start()
-
-    stage_a(0)
-    stage_a(1)
-    stage_b(0)
-
-    def body(i, carry):
-        stage_a(i)
-        send_c(i - 2)
-        stage_b(i - 1)
-        return carry
-
-    lax.fori_loop(2, g.nk, body, 0)
-    send_c(last - 1)
-    stage_b(last)
-    total = stage_c(last)
-    for i in range(last):
-        copy_c(i).wait_recv()
-        total = total + in_k[i].astype(F32)
-    for i in range(g.nk):
-        for xx in range(g.nx):
-            copy_a(i, xx).wait_send()
-        for dx in range(1, g.nx):
-            copy_b(i, dx).wait_send()
-        if i < last:
-            copy_c(i).wait_send()
-    return total
+    return ref.at[:, lanes(block, width)]
 
 
 def ff_scratch(nk, nt, rows, depth, units):
-    nx = nt // CORES
     dma = pltpu.SemaphoreType.DMA
+    blocks = nk * nt
     weights = [
-        pltpu.VMEM((units, depth), BF16),
-        pltpu.VMEM((units, depth), BF16),
-        pltpu.VMEM((units, depth), BF16),
-        dma((3,)),
+        pltpu.VMEM((CORES * units, depth), BF16),
+        pltpu.VMEM((CORES * units, depth // CORES), BF16),
+        dma((2,)),
+        dma((blocks // CORES,)),
+        dma((blocks // CORES,)),
+        dma((blocks // CORES,)),
     ]
-    gather = [
-        pltpu.VMEM((rows, depth), BF16),
-        dma((nk,)),
-        dma((nk, nx)),
-        dma((nk, nx)),
-        dma((nk * nt,)),
+    gather = [pltpu.VMEM((rows, depth), BF16), dma((blocks,)), dma((blocks,))]
+    mid = [
+        pltpu.VMEM((2 * units, rows), F32),
+        pltpu.VMEM((rows, LANES), F32),
+        pltpu.VMEM((CORES * units, rows), BF16),
+        dma((1,)),
+        dma((1,)),
     ]
-    mid = [pltpu.VMEM((rows, units), F32), pltpu.VMEM((rows, units), F32), pltpu.VMEM((rows, units), BF16)]
     scatter = [
-        pltpu.VMEM((rows, depth), BF16),
-        pltpu.VMEM((nk, nx, rows, LANES), BF16),
-        pltpu.VMEM((nk, nx - 1, rows, LANES), BF16),
-        pltpu.VMEM((nk, nx - 1, rows, LANES), BF16),
-        pltpu.VMEM((2, rows, LANES), F32),
-        pltpu.VMEM((nk - 1, rows, LANES), BF16),
-        pltpu.VMEM((nk - 1, rows, LANES), BF16),
-        dma((nk, nx)),
-        dma((nk, nx)),
-        dma((nk, nx - 1)),
-        dma((nk, nx - 1)),
-        dma((nk - 1,)),
-        dma((nk - 1,)),
+        pltpu.VMEM((LINE, rows, PLANE * LANES), F32),
+        pltpu.VMEM((LINE, 2, rows, LANES), BF16),
+        pltpu.VMEM((LINE, 2, rows, LANES), BF16),
+        pltpu.VMEM((LINE, rows, LANES), BF16),
+        pltpu.VMEM((LINE, rows, LANES), BF16),
+        pltpu.VMEM((LINE - 1, rows, LANES), BF16),
+        pltpu.VMEM((LINE - 1, rows, LANES), BF16),
+        dma((LINE, 2)),
+        dma((LINE, 2)),
+        dma((LINE,)),
+        dma((LINE,)),
+        dma((LINE - 1,)),
+        dma((LINE - 1,)),
     ]
     return weights + gather + mid + scatter
 
 
-N_FF = 4 + 5 + 3 + 13
+N_FF = 6 + 3 + 5 + 13
 
 
 def load_weights(hbm, vmem, sem):
@@ -361,27 +265,233 @@
     return copies
 
 
-def run_ff(g, own_ref, gain_ref, loads, ff):
-    wg, wu, wd, _ = ff[:4]
-    full, send_k, send_x, send_c, recv = ff[4:9]
-    acc_g, acc_u, hidden = ff[9:12]
-    gather_all(g, own_ref, full, send_k, send_x, send_c, recv)
-    loads[0].wait()
-    loads[1].wait()
-    hidden_units(full, gain_ref, wg, wu, acc_g, acc_u, hidden, full.shape[1] // g.nk)
-    loads[2].wait()
-    total = down_scatter(g, hidden, wd, *ff[12:])
-    return own_ref[...].astype(F32) + 0.5 * total
+class FeedForward:
+    def __init__(self, g, gain, wg_h, wu_h, wd_h, scratch):
+        self.g, self.gain, self.wd_h = g, gain, wd_h
+        self.wgu, self.wd, self.gu_sem, self.wl, self.ws, self.wr = scratch[:6]
+        self.full, self.send, self.recv = scratch[6:9]
+        self.acc, self.sq, self.h2, self.hs, self.hr = scratch[9:14]
+        self.scatter = scratch[14:]
+        units = wg_h.shape[0]
+        self.units = units
+        self.gu_loads = [
+            pltpu.make_async_copy(wg_h, self.wgu.at[pl.ds(0, units)], self.gu_sem.at[0]),
+            pltpu.make_async_copy(wu_h, self.wgu.at[pl.ds(units, units)], self.gu_sem.at[1]),
+        ]
+        self.own_rows = pl.ds(pl.multiple_of(g.c * units, 16), units)
+
+    def load_gate_up(self):
+        for copy in self.gu_loads:
+            copy.start()
+
+    def down_local(self, q):
+        src = cols(self.wd_h, q * CORES + self.g.c)
+        return pltpu.make_async_copy(src, self.wd.at[self.own_rows, lanes(q)], self.wl.at[q])
+
+    def down_remote(self, q):
+        g = self.g
+        src = cols(self.wd_h, q * CORES + g.oc)
+        return remote(src, self.wd.at[self.own_rows, lanes(q)], self.ws.at[q], self.wr.at[q], g.kv, g.x * CORES + g.oc)
+
+    def each(self, act):
+        def body(q, carry):
+            act(q)
+            return carry
+
+        lax.fori_loop(0, self.wd.shape[1] // LANES, body, 0)
+
+    def load_down_own(self):
+        self.each(lambda q: self.down_local(q).start())
+
+    def send_down(self):
+        self.each(lambda q: self.down_remote(q).start())
+
+    def wait_down(self):
+        def act(q):
+            self.down_local(q).wait()
+            self.down_remote(q).wait_recv()
+
+        self.each(act)
+
+    def gather(self, own_ref):
+        g, full, recv = self.g, self.full, self.recv
+        sends = Sends()
+
+        def put(src, block, z, yx, c, when=None):
+            k, t = g.at(z, yx, c)
+            copy = remote(src, cols(full, block), self.send.at[len(sends.started)], recv.at[block], k, t)
+            sends.start(copy, when)
+
+        def arrived(block):
+            remote(own_ref, cols(full, block), self.send.at[0], recv.at[block], g.kv, g.tp).wait_recv()
+
+        def sibling(src, block):
+            put(src, block, g.z, g.own, g.oc)
+
+        def line(z, other):
+            block = g.block(z, g.own, g.c)
+            arrived(block)
+            src = cols(full, block)
+            put(src, block, g.z, g.b, g.c)
+            put(src, block, g.z, g.a, g.c)
+            if other is not None:
+                put(src, block, other, g.own, g.c, g.mid)
+            sibling(src, block)
+
+        def from_a(z):
+            block = g.block(z, g.a, g.c)
+            arrived(block)
+            put(cols(full, block), block, g.z, g.b, g.c)
+            sibling(cols(full, block), block)
+
+        def last(z, yx):
+            block = g.block(z, yx, g.c)
+            arrived(block)
+            sibling(cols(full, block), block)
+
+        half = PLANE * CORES * LANES // 2
+
+        def product(z):
+            for yy in range(SIDE):
+                for xx in range(SIDE):
+                    arrived(g.block(z, (yy, xx), g.oc))
+            for part in range(2):
+                at = lanes(z * 2 + part, half)
+                x = full[:, at].astype(F32)
+                u = (x * self.gain[:, at]).astype(BF16)
+                self.acc[...] += lax.dot_general(self.wgu[:, at], u, LAST, preferred_element_type=F32)
+                x2 = x * x
+                total = self.sq[...]
+                for i in range(half // LANES):
+                    total = total + x2[:, i * LANES : (i + 1) * LANES]
+                self.sq[...] = total
+
+        mine = g.block(g.z, g.own, g.c)
+        put(own_ref, mine, g.z1, g.own, g.c)
+        put(own_ref, mine, g.z3, g.own, g.c)
+        put(own_ref, mine, g.z, g.a, g.c)
+        put(own_ref, mine, g.z, g.b, g.c)
+        sibling(own_ref, mine)
+        self.send_down()
+        full[:, lanes(mine)] = own_ref[...]
+        self.acc[...] = jnp.zeros_like(self.acc)
+        self.sq[...] = jnp.zeros_like(self.sq)
+        line(g.z1, g.z3)
+        from_a(g.z)
+        last(g.z, g.b)
+        line(g.z3, g.z1)
+        from_a(g.z1)
+        last(g.z1, g.b)
+        last(g.z, g.diag)
+        line(g.z2, None)
+        for copy in self.gu_loads:
+            copy.wait()
+        product(g.z)
+        from_a(g.z3)
+        last(g.z3, g.b)
+        last(g.z1, g.diag)
+        product(g.z1)
+        from_a(g.z2)
+        last(g.z2, g.b)
+        last(g.z3, g.diag)
+        last(g.z2, g.diag)
+        product(g.z3)
+        product(g.z2)
+        return sends
+
+    def hidden(self):
+        g, units = self.g, self.units
+        squares = jnp.sum(self.sq[...].T, axis=0, keepdims=True)
+        scale = lax.rsqrt(squares / self.full.shape[1] + epsilon)
+        gate, up = scale * self.acc[:units], scale * self.acc[units:]
+        self.h2[self.own_rows] = (jax.nn.silu(gate) * up).astype(BF16)
+        mine = self.h2.at[self.own_rows]
+        copy = remote(mine, mine, self.hs.at[0], self.hr.at[0], g.kv, g.x * CORES + g.oc)
+        copy.start()
+        self.wait_down()
+        copy.wait_recv()
+        return copy
+
+    def down(self, sends):
+        g = self.g
+        part, outb, inb, outa, ina, outz, inz, sb, rb, sa, ra, sz, rz = self.scatter
+        order = (g.z2, g.z3, g.z1, g.z)
+        width = PLANE * LANES
+
+        def own_part(i, yx):
+            return part[i, :, lanes(yx[0] * SIDE + yx[1])]
+
+        def copy_b(i, j):
+            k, t = g.at(g.z, g.b, g.c)
+            return remote(outb.at[i, j], inb.at[i, j], sb.at[i, j], rb.at[i, j], k, t)
+
+        def copy_a(i):
+            k, t = g.at(g.z, g.a, g.c)
+            return remote(outa.at[i], ina.at[i], sa.at[i], ra.at[i], k, t)
+
+        def copy_z(i):
+            k, t = g.at(order[i], g.own, g.c)
+            return remote(outz.at[i], inz.at[i], sz.at[i], rz.at[i], k, t)
+
+        def multiply(i):
+            part[i] = lax.dot_general(self.h2[...], self.wd[:, lanes(order[i], width)], FIRST, preferred_element_type=F32)
+            for j, yx in enumerate((g.diag, g.b)):
+                outb[i, j] = own_part(i, yx).astype(BF16)
+                sends.start(copy_b(i, j))
+
+        def across_a(i):
+            copy_b(i, 0).wait_recv()
+            outa[i] = (own_part(i, g.a) + inb[i, 0].astype(F32)).astype(BF16)
+            sends.start(copy_a(i))
+
+        def total(i):
+            copy_b(i, 1).wait_recv()
+            copy_a(i).wait_recv()
+            return own_part(i, g.own) + inb[i, 1].astype(F32) + ina[i].astype(F32)
+
+        def along_z(i):
+            outz[i] = total(i).astype(BF16)
+            sends.start(copy_z(i))
+
+        last = LINE - 1
+        for i in range(LINE):
+            multiply(i)
+        across_a(0)
+        for i in range(last):
+            across_a(i + 1)
+            along_z(i)
+        out = total(last)
+        for i in range(last):
+            copy_z(i).wait_recv()
+            out = out + inz[i].astype(F32)
+        return out
+
+    def run(self, own_ref):
+        with jax.named_scope("gather"):
+            sends = self.gather(own_ref)
+        with jax.named_scope("hidden"):
+            exchange = self.hidden()
+        with jax.named_scope("down"):
+            total = self.down(sends)
+        sends.started.append((exchange, None))
+        self.sends = sends
+        return own_ref[...].astype(F32) + 0.5 * total
+
+    def finish(self):
+        self.sends.finish()
+        self.each(lambda q: self.down_remote(q).wait_send())
 
 
 def first_kernel(nk, nt, tok, gain, mgain, wg_h, wu_h, wd_h, q_h, f_h, v_h, o_h, first, projected, *scratch):
     g = Grid(nk, nt)
     ff, rest = scratch[:N_FF], scratch[N_FF:]
     mixw, mix_sem, block, bsend, brecv, normed, proj, mate_got, sums, got, sq, sq_got, msend, mrecv, psend, precv, qsend, qrecv = rest
-    loads = load_weights((wg_h, wu_h, wd_h), ff[:3], ff[3])
+    block_ff = FeedForward(g, gain, wg_h, wu_h, wd_h, ff)
+    block_ff.load_gate_up()
+    block_ff.load_down_own()
     mix_loads = load_weights((q_h, f_h, v_h, o_h), [mixw.at[i] for i in range(4)], mix_sem)
     barrier(g)
-    first[...] = run_ff(g, tok, gain, loads, ff).astype(BF16)
+    first[...] = block_ff.run(tok).astype(BF16)
 
     copies = []
     for step in range(1, nt):
@@ -448,6 +558,7 @@
             p_copy(i, dz).wait_recv()
             total = total + got[i, dz - 1].astype(F32)
         projected[:, i * inner : (i + 1) * inner] = total * scale
+    block_ff.finish()
     for copy in copies:
         copy.wait_send()
     for step in range(1, nk):
@@ -510,7 +621,9 @@
     ff, rest = scratch[:N_FF], scratch[N_FF:]
     po, po_sem, yfull, ysend, yrecv, part, got, tsend, trecv, second = rest
     po_load = load_weights((po_h,), (po,), po_sem)
-    loads = load_weights((wg_h, wu_h, wd_h), ff[:3], ff[3])
+    block_ff = FeedForward(g, gain, wg_h, wu_h, wd_h, ff)
+    block_ff.load_gate_up()
+    block_ff.load_down_own()
     barrier(g)
     own_rows = y.shape[0]
 
@@ -538,7 +651,8 @@
         t_copy(step).wait_recv()
         total = total + got[step - 1].astype(F32)
     second[...] = (first[...].astype(F32) + total).astype(BF16)
-    result[...] = run_ff(g, second, gain, loads, ff).astype(BF16)
+    result[...] = block_ff.run(second).astype(BF16)
+    block_ff.finish()
     for step in range(1, nk):
         y_copy(step, g.k(step), g.kv).wait_send()
     for step in range(1, nt):
@@ -649,7 +763,7 @@
         P(None, ("kv", "tp")),
         P(("kv", "tp"), None),
     )
-    blocks_fit = D == mesh.shape["kv"] * mesh.shape["tp"] * LANES and mesh.shape["tp"] >= 2 * CORES
+    blocks_fit = D == mesh.shape["kv"] * mesh.shape["tp"] * LANES and mesh.shape["tp"] == SIDE * CORES and mesh.shape["kv"] == LINE * SIDE
     return jax.shard_map(
         per_device if blocks_fit else per_device_plain,
         mesh=mesh,

time: 174 us -> 132 us (0.76)
  Pallas kernels: 166 us -> 125 us
    pallas_call x2, Pallas kernels: 155 us -> 114 us  [call(): pl.pallas_call(kernel, out_shape=outs, in_specs=[vmem] * n_vmem + [any_sp...]
where the time goes in v1:
time: 132 us
  Pallas kernels  125 us (95%)
  local copies, waits for them, and re-layouts  6.42 us (5%)
    pallas_call x2, Pallas kernels, call(): pl.pallas_call(kernel, out_shape=outs, in_specs=[vmem] * n_vmem + [any_sp...  114 us
    pallas_call x1, Pallas kernels, recurrence(): pl.pallas_call(recurrence_kernel, grid=(rows // step,), out_shape=(jax.Sh...  10.7 us
    unnamed x11, local copies, waits for them, and re-layouts  6.42 us

profile of v1, /device:TPU:0, one launch (start us, length us, event | category | flops | bytes accessed | tf_op | source)
XLA Modules:
  0.0 131.9 jit_solution(7225540832264300608)
XLA Ops:
  0.6 0.0 copy-start.3
  0.6 0.0 copy-start.4
  0.7 64.3 %shard_map.185 = (bf16[256,128]{1,0:T(8,128)(2,1)}, f32[32,2048]{1,0:T(8,128)}) custom-call(bf16[256,128]{1,0:T(8,128)(2,1)} %tok.1, f32[1,4096]{1,0:T(1,128)} %bitcast.15, f32[1,4096]{1,0:T(1,128)} %bitcast.16, bf16[352,4096]{1,0:T(8,128)(2,1)} %bitcast.11, bf16[352,4096]{1,0:T(8,128)(2,1)} %bitcast.12, bf16[352,4096]{1,0:T(8,128)(2,1)} %wd_h.2, ...), custom_call_target="tpu_custom_call" | custom-call | tf_op jit(solution)/shard_map/pallas_call | solution.py:664
  65.0 0.0 copy-done.3
  65.0 0.0 copy-done.4
  65.0 0.0 copy-start
  65.0 3.4 %copy-done = f32[32,4,128,128]{3,2,1,0:T(8,128)S(1)} copy-done((f32[32,4,128,128]{3,2,1,0:T(8,128)S(1)}, f32[32,4,128,128]{3,2,1,0:T(8,128)}, u32[]{:S(2)}) %copy-start) | copy-done | bytes 8388632
  68.4 0.0 copy-start.1
  68.4 0.9 copy-done.1
  69.3 10.7 %shard_map.186 = (f32[32,4,128,128]{3,2,1,0:T(8,128)}, bf16[32,512]{1,0:T(8,128)(2,1)S(1)}) custom-call(f32[32,2048]{1,0:T(8,128)S(1)} %copy-done.1, f32[32,4,128,128]{3,2,1,0:T(8,128)S(1)} %copy-done, f32[1,512]{1,0:T(1,128)S(1)} %bitcast.9, f32[1,128]{1,0:T(1,128)S(1)} %bitcast.10), custom_call_target="tpu_custom_call" | custom-call | tf_op jit(solution)/shard_map/pallas_call | solution.py:601
  80.0 0.0 copy-start.2
  80.0 0.6 copy-done.2
  80.6 49.8 %shard_map.187 = bf16[256,128]{1,0:T(8,128)(2,1)} custom-call(bf16[32,512]{1,0:T(8,128)(2,1)} %copy-done.2, bf16[256,128]{1,0:T(8,128)(2,1)} %get-tuple-element.8.first, f32[1,4096]{1,0:T(1,128)} %bitcast.17, bf16[512,512]{1,0:T(8,128)(2,1)} %po_h.1, bf16[352,4096]{1,0:T(8,128)(2,1)} %bitcast.13, bf16[352,4096]{1,0:T(8,128)(2,1)} %bitcast.14, ...), custom_call_target="tpu_custom_call" | custom-call | tf_op jit(solution)/shard_map/pallas_call | solution.py:664
  130.4 1.5 %copy.21 = bf16[256,128]{1,0:T(8,128)(2,1)} copy(bf16[256,128]{1,0:T(8,128)(2,1)} %shard_map.187) | data formatting | bytes 131072
Async XLA Ops:
  0.6 64.3 %copy-start.3 = (f32[512]{0:T(512)S(1)}, f32[512]{0:T(512)}, u32[]{:S(2)}) copy-start(f32[512]{0:T(512)} %param.29) | copy-start | bytes 6148
  0.6 64.3 %copy-start.4 = (f32[128]{0:T(128)S(1)}, f32[128]{0:T(128)}, u32[]{:S(2)}) copy-start(f32[128]{0:T(128)} %param.30) | copy-start | bytes 1540
  65.0 3.4 %copy-start = (f32[32,4,128,128]{3,2,1,0:T(8,128)S(1)}, f32[32,4,128,128]{3,2,1,0:T(8,128)}, u32[]{:S(2)}) copy-start(f32[32,4,128,128]{3,2,1,0:T(8,128)} %past.1) | copy-start | bytes 25165828
  68.4 0.9 copy-start.1
  80.0 0.6 copy-start.2

commit v2 on v1

v2 whole, which is shorter than its diff:
```python
import functools

import jax
import jax.numpy as jnp
from jax import lax
from jax.experimental import pallas as pl
from jax.experimental.pallas import tpu as pltpu
from jax.sharding import PartitionSpec as P

D = 4096


epsilon = 1e-06


def half_inputs(activations, gain, w_gate, w_up):
    piece_float = lax.all_gather(activations, ("kv", "tp"), axis=1, tiled=True).astype(jnp.float32)
    normed = (piece_float * gain).astype(jnp.bfloat16)
    gate_acc = jnp.dot(normed, w_gate, preferred_element_type=jnp.float32)
    up_acc = jnp.dot(normed, w_up, preferred_element_type=jnp.float32)
    squares = jnp.sum(piece_float * piece_float, axis=1)
    row_scale = lax.rsqrt(squares / D + epsilon)[:, None]
    return (jax.nn.silu(row_scale * gate_acc) * (row_scale * up_acc)).astype(jnp.bfloat16)


def down_sum(hidden, w_down):
    return lax.psum_scatter(
        jnp.dot(hidden, w_down, preferred_element_type=jnp.float32),
        ("kv", "tp"),
        scatter_dimension=1,
        tiled=True,
    )


def per_device_plain(
    tokens,
    past_state,
    pre_gain,
    pre_gate,
    pre_up,
    pre_down,
    mix_gain,
    query_weight,
    forget_weight,
    value_weight,
    output_gate_weight,
    forget_floor,
    head_gain,
    proj_out,
    post_gain,
    post_gate,
    post_up,
    post_down,
):
    whole_rows = lax.all_gather(tokens, ("kv", "tp"), axis=1, tiled=True)
    whole_float = whole_rows.astype(jnp.float32)
    row_scale = lax.rsqrt(jnp.mean(whole_float * whole_float, axis=1, keepdims=True) + epsilon)
    normed = (whole_float * pre_gain).astype(jnp.bfloat16)
    gate_pre = row_scale * jnp.dot(normed, pre_gate, preferred_element_type=jnp.float32)
    up_pre = row_scale * jnp.dot(normed, pre_up, preferred_element_type=jnp.float32)
    hidden = (jax.nn.silu(gate_pre) * up_pre).astype(jnp.bfloat16)
    kv_sums = lax.psum_scatter(
        jnp.dot(hidden, pre_down, preferred_element_type=jnp.float32).astype(jnp.bfloat16),
        "kv",
        scatter_dimension=1,
        tiled=True,
    )
    block_sum = lax.psum(kv_sums, "tp").astype(jnp.float32)
    block_width = block_sum.shape[1]
    block_old = lax.dynamic_slice_in_dim(
        whole_rows, lax.axis_index("kv") * block_width, block_width, 1
    )
    block_rows = (block_old.astype(jnp.float32) + 0.5 * block_sum).astype(jnp.bfloat16)
    own_width = block_width // lax.axis_size("tp")
    after_first = lax.dynamic_slice_in_dim(
        block_rows, lax.axis_index("tp") * own_width, own_width, 1
    )
    block_width = block_rows.shape[1]
    block_float = block_rows.astype(jnp.float32)
    block_gain = lax.dynamic_slice_in_dim(
        mix_gain, lax.axis_index("kv") * block_width, block_width, 0
    )
    squares = lax.psum(jnp.sum(block_float * block_float, axis=1), "kv")
    normed = (block_float * block_gain).astype(jnp.bfloat16)
    own_rows = past_state.shape[0]
    weight_list = (query_weight, forget_weight, value_weight, output_gate_weight)
    projected = lax.psum_scatter(
        jnp.concatenate(
            [
                jnp.dot(normed, weight_part, preferred_element_type=jnp.float32)
                for weight_part in weight_list
            ],
            axis=1,
        ).astype(jnp.bfloat16),
        "kv",
        scatter_dimension=0,
        tiled=True,
    ).astype(jnp.float32)
    own_squares = lax.dynamic_slice_in_dim(squares, lax.axis_index("kv") * own_rows, own_rows, 0)
    projected = projected * lax.rsqrt(own_squares / D + epsilon)[:, None]
    pre_query, pre_forget, pre_value, pre_gate_out = jnp.split(projected, 4, axis=1)
    local_heads = past_state.shape[1]
    head_width = past_state.shape[2]
    head_shape = (own_rows, local_heads, head_width)
    floors = forget_floor.reshape(local_heads, head_width)
    forget_heads = pre_forget.reshape(head_shape)
    forget = floors + (1.0 - floors) * jax.nn.sigmoid(forget_heads)
    written = (1.0 - floors) * jax.nn.sigmoid(-forget_heads)
    query_act = jax.nn.silu(pre_query.reshape(head_shape))
    value_act = pre_value.reshape(head_shape)
    new_state = (
        forget[:, :, :, None] * past_state + written[:, :, :, None] * value_act[:, :, None, :]
    )
    readout = jnp.einsum("bhkv,bhk->bhv", new_state, query_act, precision=lax.Precision.HIGHEST)
    readout = (
        readout
        * lax.rsqrt(jnp.mean(readout * readout, axis=2, keepdims=True) + epsilon)
        * head_gain
    )
    mixed_in = (
        readout.reshape(own_rows, local_heads * head_width) * jax.nn.silu(pre_gate_out)
    ).astype(jnp.bfloat16)
    partials = jnp.dot(
        lax.all_gather(mixed_in, "kv", axis=0, tiled=True),
        proj_out,
        preferred_element_type=jnp.float32,
    ).astype(jnp.bfloat16)
    mixed_sum = lax.psum_scatter(partials, "tp", scatter_dimension=1, tiled=True).astype(
        jnp.float32
    )
    second = (after_first.astype(jnp.float32) + mixed_sum).astype(jnp.bfloat16)
    hidden_two = half_inputs(second, post_gain, post_gate, post_up)
    result = (second.astype(jnp.float32) + 0.5 * down_sum(hidden_two, post_down)).astype(
        jnp.bfloat16
    )
    return (result, new_state)


LANES = 128
LAST = (((1,), (1,)), ((), ()))
FIRST = (((0,), (0,)), ((), ()))
CORES, LINE, SIDE = 2, 4, 2
PLANE = SIDE * SIDE
F32, BF16 = jnp.float32, jnp.bfloat16
MESH = pl.DeviceIdType.MESH


class Grid:
    def __init__(self, n_kv, n_tp):
        self.nk, self.nt = n_kv, n_tp
        self.kv, self.tp = lax.axis_index("kv"), lax.axis_index("tp")
        self.z, self.y = self.kv // SIDE, self.kv % SIDE
        self.x, self.c = self.tp // CORES, self.tp % CORES
        self.oc = 1 - self.c
        y, x, c = self.y, self.x, self.c
        self.own = (y, x)
        self.a = (y + c * (1 - 2 * y), x + (1 - c) * (1 - 2 * x))
        self.b = (y + (1 - c) * (1 - 2 * y), x + c * (1 - 2 * x))
        self.diag = (1 - y, 1 - x)
        self.z1 = self.z + 1 - 2 * (self.z % 2)
        self.z3 = LINE - 1 - self.z
        self.z2 = LINE - 1 - self.z1
        self.mid = (self.z == 1) | (self.z == 2)

    def k(self, step):
        return lax.rem(self.kv + step, self.nk)

    def t(self, step):
        return lax.rem(self.tp + step, self.nt)

    def block(self, z, yx, c):
        return (z * SIDE + yx[0]) * self.nt + yx[1] * CORES + c

    def z_of(self, block):
        return block // self.nt

    def at(self, z, yx, c):
        return z * SIDE + yx[0], yx[1] * CORES + c


def remote(src, dst, send, recv, k, t):
    return pltpu.make_async_remote_copy(
        src_ref=src, dst_ref=dst, send_sem=send, recv_sem=recv,
        device_id={"kv": k, "tp": t}, device_id_type=MESH,
    )


def start(copy, when=None):
    if when is None:
        copy.start()
    else:
        pl.when(when)(copy.start)


def drain(ref, sem):
    pltpu.make_async_copy(ref, ref, sem).wait()


def greet(g):
    sem = pltpu.get_barrier_semaphore()
    for step in range(1, g.nk):
        pl.semaphore_signal(sem, inc=1, device_id={"kv": g.k(step), "tp": g.tp}, device_id_type=MESH)
    for step in range(1, g.nt):
        pl.semaphore_signal(sem, inc=1, device_id={"kv": g.kv, "tp": g.t(step)}, device_id_type=MESH)
    k, t = g.at(g.z, g.diag, g.c)
    pl.semaphore_signal(sem, inc=1, device_id={"kv": k, "tp": t}, device_id_type=MESH)


def barrier(g):
    pl.semaphore_wait(pltpu.get_barrier_semaphore(), g.nk - 1 + g.nt - 1 + 1)


def lanes(index, width=LANES):
    return pl.ds(pl.multiple_of(index * width, LANES), width)


def cols(ref, block, width=LANES):
    return ref.at[:, lanes(block, width)]


def ff_scratch(nk, nt, rows, depth, units):
    dma = pltpu.SemaphoreType.DMA
    blocks = nk * nt
    weights = [
        pltpu.VMEM((CORES * units, depth), BF16),
        pltpu.VMEM((CORES * units, depth // CORES), BF16),
        dma((2,)),
        dma((3,)),
    ]
    gather = [pltpu.VMEM((rows, depth), BF16), dma((3,)), dma((blocks // CORES,)), dma((blocks // CORES,)), dma((nk,))]
    mid = [
        pltpu.VMEM((2 * units, rows), F32),
        pltpu.VMEM((rows, LANES), F32),
        pltpu.VMEM((CORES * units, rows), BF16),
        dma((1,)),
        dma((1,)),
    ]
    scatter = [
        pltpu.VMEM((LINE, rows, PLANE * LANES), F32),
        pltpu.VMEM((LINE, 2, rows, LANES), BF16),
        pltpu.VMEM((LINE, 2, rows, LANES), BF16),
        pltpu.VMEM((LINE, rows, LANES), BF16),
        pltpu.VMEM((LINE, rows, LANES), BF16),
        pltpu.VMEM((LINE - 1, rows, LANES), BF16),
        pltpu.VMEM((LINE - 1, rows, LANES), BF16),
        dma((1,)),
        dma((LINE, 2)),
        dma((LINE,)),
        dma((LINE - 1,)),
    ]
    return weights + gather + mid + scatter


N_FF = 4 + 5 + 5 + 11


def load_weights(hbm, vmem, sem):
    copies = [pltpu.make_async_copy(a, b, sem.at[i]) for i, (a, b) in enumerate(zip(hbm, vmem))]
    for copy in copies:
        copy.start()
    return copies


class FeedForward:
    def __init__(self, g, gain, wg_h, wu_h, wd_h, scratch):
        self.g, self.gain, self.wd_h = g, gain, wd_h
        self.wgu, self.wd, self.gu_sem, self.wd_sem = scratch[:4]
        self.full, self.send, self.recv, self.recv_low, self.recv_core = scratch[4:9]
        self.acc, self.sq, self.h2, self.hs, self.hr = scratch[9:14]
        self.scatter = scratch[14:]
        units = wg_h.shape[0]
        self.units = units
        self.sent_down = False
        self.gu_loads = [
            pltpu.make_async_copy(wg_h, self.wgu.at[pl.ds(0, units)], self.gu_sem.at[0]),
            pltpu.make_async_copy(wu_h, self.wgu.at[pl.ds(units, units)], self.gu_sem.at[1]),
        ]
        self.own_rows = pl.ds(pl.multiple_of(g.c * units, 16), units)

    def load_gate_up(self):
        for copy in self.gu_loads:
            copy.start()

    def down_local(self, q):
        src = cols(self.wd_h, q * CORES + self.g.c)
        return pltpu.make_async_copy(src, self.wd.at[self.own_rows, lanes(q)], self.wd_sem.at[0])

    def down_remote(self, q):
        g = self.g
        src = cols(self.wd_h, q * CORES + g.oc)
        dst = self.wd.at[self.own_rows, lanes(q)]
        return remote(src, dst, self.wd_sem.at[1], self.wd_sem.at[2], g.kv, g.x * CORES + g.oc)

    def each(self, act):
        def body(q, carry):
            act(q)
            return carry

        lax.fori_loop(0, self.wd.shape[1] // LANES, body, 0)

    def load_down_own(self):
        self.each(lambda q: self.down_local(q).start())

    def send_down(self):
        self.sent_down = True
        self.each(lambda q: self.down_remote(q).start())

    def wait_down(self):
        drain(self.wd.at[self.own_rows], self.wd_sem.at[0])
        drain(self.wd.at[self.own_rows], self.wd_sem.at[2])

    def gather(self, own_ref):
        g, full = self.g, self.full
        rows = full.shape[0]
        cut = rows * 3 // 4
        whole, upper, lower = slice(0, rows), slice(0, cut), slice(cut, rows)
        sizes = (whole, upper, lower)
        always, inner = [0, 0, 0], [0, 0, 0]

        def put(src, block, at, z, yx, c, when=None):
            k, t = g.at(z, yx, c)
            dst = full.at[at, lanes(block)]
            kind = sizes.index(at)
            if c is g.oc:
                recv = self.recv_core.at[g.z_of(block)]
            else:
                recv = (self.recv_low if at is lower else self.recv).at[block // CORES]
            start(remote(dst if src is None else src, dst, self.send.at[kind], recv, k, t), when)
            (always if when is None else inner)[kind] += 1

        def arrived(block, at):
            drain(full.at[at, lanes(block)], (self.recv_low if at is lower else self.recv).at[block // CORES])

        def line(z, other):
            block = g.block(z, g.own, g.c)
            arrived(block, whole)
            if other is not None:
                put(None, block, whole, other, g.own, g.c, g.mid)
            else:
                put(None, block, upper, g.z, g.diag, g.c)
            put(None, block, upper, g.z, g.b, g.c)
            put(None, block, upper, g.z, g.a, g.c)
            put(None, block, whole, g.z, g.own, g.oc)

        def plane(yx):
            block = g.block(g.z, yx, g.c)
            arrived(block, whole)
            put(None, block, lower, g.z1, g.own, g.c)
            put(None, block, lower, g.z3, g.own, g.c)
            put(None, block, whole, g.z, g.own, g.oc)

        def from_a(z):
            block = g.block(z, g.a, g.c)
            arrived(block, upper)
            put(None, block, upper, g.z, g.b, g.c)
            put(None, block, upper, g.z, g.own, g.oc)

        def last(z, yx):
            block = g.block(z, yx, g.c)
            arrived(block, upper)
            put(None, block, upper, g.z, g.own, g.oc)

        def low(z, yx, other=None):
            block = g.block(z, yx, g.c)
            arrived(block, lower)
            if other is not None:
                put(None, block, lower, other, g.own, g.c, g.mid)
            put(None, block, lower, g.z, g.own, g.oc)

        half = SIDE * CORES * LANES

        def product(z, y):
            drain(full.at[:, lanes(z * SIDE + y, half // CORES)], self.recv_core.at[z * SIDE + y])
            at = lanes(z * SIDE + y, half)
            x = full[:, at].astype(F32)
            u = (x * self.gain[:, at]).astype(BF16)
            self.acc[...] += lax.dot_general(self.wgu[:, at], u, LAST, preferred_element_type=F32)
            x2 = x * x
            total = self.sq[...]
            for i in range(half // LANES):
                total = total + x2[:, i * LANES : (i + 1) * LANES]
            self.sq[...] = total

        oy = 1 - g.y
        mine = g.block(g.z, g.own, g.c)
        put(own_ref, mine, whole, g.z1, g.own, g.c)
        put(own_ref, mine, whole, g.z3, g.own, g.c)
        put(own_ref, mine, whole, g.z, g.a, g.c)
        put(own_ref, mine, whole, g.z, g.b, g.c)
        put(own_ref, mine, whole, g.z, g.diag, g.c)
        put(own_ref, mine, whole, g.z, g.own, g.oc)
        full[:, lanes(mine)] = own_ref[...]
        self.acc[...] = jnp.zeros_like(self.acc)
        self.sq[...] = jnp.zeros_like(self.sq)
        line(g.z1, g.z3)
        plane(g.a)
        plane(g.b)
        line(g.z3, g.z1)
        plane(g.diag)
        from_a(g.z1)
        last(g.z1, g.b)
        low(g.z1, g.a, g.z3)
        low(g.z1, g.b, g.z3)
        line(g.z2, None)
        if not self.sent_down:
            self.send_down()
        from_a(g.z3)
        last(g.z3, g.b)
        low(g.z3, g.a, g.z1)
        low(g.z3, g.b, g.z1)
        low(g.z1, g.diag, g.z3)
        last(g.z1, g.diag)
        for copy in self.gu_loads:
            copy.wait()
        product(g.z, g.y)
        low(g.z3, g.diag, g.z1)
        last(g.z3, g.diag)
        last(g.z2, g.a)
        last(g.z2, g.b)
        product(g.z, oy)
        product(g.z1, g.y)
        low(g.z2, g.a)
        low(g.z2, g.b)
        product(g.z1, oy)
        product(g.z3, g.y)
        last(g.z2, g.diag)
        low(g.z2, g.diag)
        product(g.z3, oy)
        product(g.z2, g.y)
        product(g.z2, oy)
        self.sent = list(zip(sizes, always, inner))

    def hidden(self):
        g, units = self.g, self.units
        squares = jnp.sum(self.sq[...].T, axis=0, keepdims=True)
        scale = lax.rsqrt(squares / self.full.shape[1] + epsilon)
        gate, up = scale * self.acc[:units], scale * self.acc[units:]
        self.h2[self.own_rows] = (jax.nn.silu(gate) * up).astype(BF16)
        mine = self.h2.at[self.own_rows]
        copy = remote(mine, mine, self.hs.at[0], self.hr.at[0], g.kv, g.x * CORES + g.oc)
        copy.start()
        self.wait_down()
        copy.wait_recv()
        return copy

    def down(self):
        g = self.g
        part, outb, inb, outa, ina, outz, inz, out_sem, rb, ra, rz = self.scatter
        sent = out_sem.at[0]
        order = (g.z2, g.z3, g.z1, g.z)
        width = PLANE * LANES

        def own_part(i, yx):
            return part[i, :, lanes(yx[0] * SIDE + yx[1])]

        def copy_b(i, j):
            k, t = g.at(g.z, g.b, g.c)
            return remote(outb.at[i, j], inb.at[i, j], sent, rb.at[i, j], k, t)

        def copy_a(i):
            k, t = g.at(g.z, g.a, g.c)
            return remote(outa.at[i], ina.at[i], sent, ra.at[i], k, t)

        def copy_z(i):
            k, t = g.at(order[i], g.own, g.c)
            return remote(outz.at[i], inz.at[i], sent, rz.at[i], k, t)

        def multiply(i):
            part[i] = lax.dot_general(self.h2[...], self.wd[:, lanes(order[i], width)], FIRST, preferred_element_type=F32)
            for j, yx in enumerate((g.diag, g.b)):
                outb[i, j] = own_part(i, yx).astype(BF16)
                copy_b(i, j).start()

        def across_a(i):
            copy_b(i, 0).wait_recv()
            outa[i] = (own_part(i, g.a) + inb[i, 0].astype(F32)).astype(BF16)
            copy_a(i).start()

        def total(i):
            copy_b(i, 1).wait_recv()
            copy_a(i).wait_recv()
            return own_part(i, g.own) + inb[i, 1].astype(F32) + ina[i].astype(F32)

        def along_z(i):
            outz[i] = total(i).astype(BF16)
            copy_z(i).start()

        last = LINE - 1
        for i in range(LINE):
            multiply(i)
        across_a(0)
        for i in range(last):
            across_a(i + 1)
            along_z(i)
        out = total(last)
        for i in range(last):
            copy_z(i).wait_recv()
            out = out + inz[i].astype(F32)
        return out

    def run(self, own_ref):
        with jax.named_scope("gather"):
            self.gather(own_ref)
        with jax.named_scope("hidden"):
            self.exchange = self.hidden()
        with jax.named_scope("down"):
            total = self.down()
        return own_ref[...].astype(F32) + 0.5 * total

    def finish(self):
        g, full = self.g, self.full
        self.exchange.wait_send()
        drain(self.wd.at[self.own_rows], self.wd_sem.at[1])
        drain(full.at[:, : (LINE * 4 - 1) * LANES], self.scatter[7].at[0])
        for kind, (rows, always, inner) in enumerate(self.sent):
            sem = self.send.at[kind]
            if inner:
                pl.when(g.mid)(lambda rows=rows, n=always + inner, sem=sem: drain(full.at[rows, : n * LANES], sem))
                pl.when(jnp.logical_not(g.mid))(lambda rows=rows, n=always, sem=sem: drain(full.at[rows, : n * LANES], sem))
            else:
                drain(full.at[rows, : always * LANES], sem)


def first_kernel(nk, nt, tok_h, gain_h, mgain_h, wg_h, wu_h, wd_h, q_h, f_h, v_h, o_h, first, projected, *scratch):
    g = Grid(nk, nt)
    greet(g)
    ff, rest = scratch[:N_FF], scratch[N_FF:]
    tok, gain, mgain, in_sem, mixw, mix_sem, block, bsend, brecv, normed, proj, ygot, outp, inp, outc, inc, sq, sq_got, sq_col, ys, yr, ps, pr, cs, cr, qsend, qrecv = rest
    in_loads = load_weights((tok_h, gain_h, mgain_h), (tok, gain, mgain), in_sem)
    block_ff = FeedForward(g, gain, wg_h, wu_h, wd_h, ff)
    block_ff.load_gate_up()
    block_ff.load_down_own()
    mix_loads = load_weights((q_h, f_h, v_h, o_h), [mixw.at[i] for i in range(4)], mix_sem)
    with jax.named_scope("barrier"):
        barrier(g)
        for copy in in_loads:
            copy.wait()
    first[...] = block_ff.run(tok).astype(BF16)

    rows, width = block.shape
    half = rows // 2
    far, near = 1 - g.z // 2, g.z // 2
    other = (1 - g.x) * CORES
    sib = g.x * CORES + g.oc

    def half_rows(q):
        return pl.ds(pl.multiple_of(q * half, half), half)

    def b_copy(src, index, q, t):
        dst = block.at[half_rows(q), lanes(index)]
        return remote(src, dst, bsend.at[0], brecv.at[index, q], g.kv, t)

    def b_wait(index, q):
        b_copy(first.at[half_rows(q)], index, q, sib).wait_recv()

    for q in (far, near):
        b_copy(first.at[half_rows(q)], g.tp, q, other + g.c).start()
        b_copy(first.at[half_rows(q)], g.tp, q, sib).start()
    block[:, lanes(g.tp)] = first[...]
    for q in (far, near):
        b_wait(other + g.c, q)
        b_copy(block.at[half_rows(q), lanes(other + g.c)], other + g.c, q, sib).start()
    own_rows, inner = projected.shape[0], projected.shape[1] // 4

    def normalise(q):
        b_wait(sib, q)
        b_wait(other + g.oc, q)
        x = block[half_rows(q), :].astype(F32)
        normed[half_rows(q), :] = (x * mgain[:, lanes(g.kv, width)]).astype(BF16)
        x2 = x * x
        squares = x2[:, :LANES]
        for i in range(1, width // LANES):
            squares = squares + x2[:, i * LANES : (i + 1) * LANES]
        sq[:, lanes(q, half)] = jnp.broadcast_to(jnp.sum(squares.T, axis=0, keepdims=True), (sq.shape[0], half))

    def rows_of(k):
        return pl.ds(pl.multiple_of(k * own_rows, own_rows), own_rows)

    def sq_part(k):
        return k * own_rows // LANES

    oy = 1 - g.y
    peers = ((g.z2, g.y), (g.z2, oy), (g.z3, g.y), (g.z3, oy), (g.z1, g.y), (g.z1, oy), (g.z, oy))

    def q_copy(i):
        k = peers[i][0] * SIDE + peers[i][1]
        return remote(cols(sq, sq_part(k)), sq_got.at[i], qsend.at[0], qrecv.at[0], k, g.tp)

    order = (g.z2, g.z3, g.z1, g.z)
    halves = 2
    wide = 4 * inner // halves

    def side(h):
        return slice(h * wide, (h + 1) * wide)

    def y_copy(j, h):
        src = proj.at[rows_of(order[j] * SIDE + 1 - g.y), pl.ds(h * wide, wide)]
        return remote(src, ygot.at[j, h], ys.at[0], yr.at[j, h], g.z * SIDE + 1 - g.y, g.tp)

    def p_copy(j, h):
        return remote(outp.at[j, h], inp.at[j, h], ps.at[0], pr.at[j, h], g.z1 * SIDE + g.y, g.tp)

    def c_copy(h):
        return remote(outc.at[h], inc.at[h], cs.at[0], cr.at[h], g.z3 * SIDE + g.y, g.tp)

    def y_sum(j, h):
        y_copy(j, h).wait_recv()
        return proj[rows_of(order[j] * SIDE + g.y), side(h)].astype(F32) + ygot[j, h].astype(F32)

    for copy in mix_loads:
        copy.wait()
    for part, q in enumerate((far, near)):
        with jax.named_scope("mixnorm"):
            normalise(q)
        for i in range(4) if part == 0 else range(4, nk - 1):
            q_copy(i).start()
        for h in range(halves):
            with jax.named_scope("mixdot"):
                for i in range(h * 2, h * 2 + 2):
                    out = jnp.dot(normed[half_rows(q), :], mixw[i], preferred_element_type=F32)
                    proj[half_rows(q), i * inner : (i + 1) * inner] = out.astype(BF16)
            y_copy(2 * part, h).start()
        for h in range(halves):
            y_copy(2 * part + 1, h).start()
    with jax.named_scope("mix0"):
        for h in range(halves):
            outp[0, h] = y_sum(0, h).astype(BF16)
            p_copy(0, h).start()
    with jax.named_scope("mix1"):
        for h in range(halves):
            total = y_sum(1, h)
            p_copy(0, h).wait_recv()
            outc[h] = (total + inp[0, h].astype(F32)).astype(BF16)
            c_copy(h).start()
    with jax.named_scope("mix2"):
        for h in range(halves):
            outp[1, h] = y_sum(2, h).astype(BF16)
            p_copy(1, h).start()
    with jax.named_scope("mix3"):
        squares = sq[:, lanes(sq_part(g.kv))]
        drain(sq_got, qrecv.at[0])
        for i in range(nk - 1):
            squares = squares + sq_got[i]
        sq_col[...] = jnp.broadcast_to(squares[:1], sq_col.shape).T
        mine = pl.ds(pl.multiple_of(g.kv * own_rows % LANES, own_rows), own_rows)
        scale = lax.rsqrt(sq_col[mine, :1] / mgain.shape[1] + epsilon)
        for h in range(halves):
            total = y_sum(3, h)
            p_copy(1, h).wait_recv()
            c_copy(h).wait_recv()
            projected[:, side(h)] = (total + inp[1, h].astype(F32) + inc[h].astype(F32)) * scale
    block_ff.finish()
    drain(block.at[:, : (nt - 1) * LANES], bsend.at[0])
    drain(ygot, ys.at[0])
    drain(outp, ps.at[0])
    drain(outc, cs.at[0])
    drain(sq_got, qsend.at[0])


def recurrence_kernel(projected, past, floor, head_gain, new, mixed, spread):
    rows, heads, width = past.shape[:3]
    inner = heads * width
    base = floor[...]
    forget = base + (1.0 - base) * jax.nn.sigmoid(projected[:, inner : 2 * inner])
    left = jnp.concatenate([forget, jax.nn.silu(projected[:, :inner])], axis=1)
    parts = []
    for _ in range(3):
        parts.append(left.astype(BF16).astype(F32))
        left = left - parts[-1]
    three = jnp.concatenate(parts, axis=0).astype(BF16)
    shape = (3 * rows, rows * width)
    chosen = lax.broadcasted_iota(jnp.int32, shape, 0) % rows == lax.broadcasted_iota(jnp.int32, shape, 1) // width
    spread[...] = lax.dot_general(three, chosen.astype(BF16), FIRST, preferred_element_type=F32)
    for h in range(heads):
        at = slice(h * width, (h + 1) * width)
        outs = []
        for n in range(rows):
            col = slice(n * width, (n + 1) * width)
            value = projected[n : n + 1, 2 * inner + h * width : 2 * inner + (h + 1) * width]
            state = value + spread[at, col] * (past[n, h] - value)
            new[n, h] = state
            query = spread[inner + h * width : inner + (h + 1) * width, col]
            outs.append(jnp.sum(state * query, axis=0, keepdims=True))
        read = jnp.concatenate(outs, axis=0)
        read = read * lax.rsqrt(jnp.mean(read * read, axis=1, keepdims=True) + epsilon) * head_gain[...]
        gate = projected[:, 3 * inner + h * width : 3 * inner + (h + 1) * width]
        mixed[:, at] = (read * jax.nn.silu(gate)).astype(BF16)


def recurrence(projected, past_state, forget_floor, head_gain):
    rows, heads, width = past_state.shape[:3]
    inner, step = heads * width, 8
    state_spec = pl.BlockSpec((step, heads, width, width), lambda i: (i, 0, 0, 0))
    return pl.pallas_call(
        recurrence_kernel,
        grid=(rows // step,),
        out_shape=(
            jax.ShapeDtypeStruct(past_state.shape, F32),
            jax.ShapeDtypeStruct((rows, inner), BF16),
        ),
        in_specs=[
            pl.BlockSpec((step, 4 * inner), lambda i: (i, 0)),
            state_spec,
            pl.BlockSpec((1, inner), lambda i: (0, 0)),
            pl.BlockSpec((1, width), lambda i: (0, 0)),
        ],
        out_specs=(state_spec, pl.BlockSpec((step, inner), lambda i: (i, 0))),
        scratch_shapes=[pltpu.VMEM((2 * inner, step * width), F32)],
        compiler_params=pltpu.CompilerParams(vmem_limit_bytes=32 * 1024 * 1024),
    )(projected, past_state, forget_floor[None], head_gain[None])


def second_kernel(nk, nt, y, first, gain, po_h, wg_h, wu_h, wd_h, result, *scratch):
    g = Grid(nk, nt)
    greet(g)
    ff, rest = scratch[:N_FF], scratch[N_FF:]
    po, po_sem, yfull, ysend, yrecv, part, got, tsend, trecv, second = rest
    po_load = load_weights((po_h,), (po,), po_sem)
    block_ff = FeedForward(g, gain, wg_h, wu_h, wd_h, ff)
    block_ff.load_gate_up()
    block_ff.load_down_own()
    with jax.named_scope("barrier"):
        barrier(g)
    own_rows = y.shape[0]
    oy = 1 - g.y

    def rows_of(k, count=1):
        return pl.ds(pl.multiple_of(k * own_rows * count, own_rows), own_rows * count)

    def put(src, owner, z, yy, when=None):
        start(remote(src, yfull.at[rows_of(owner)], ysend.at[0], yrecv.at[owner], z * SIDE + yy, g.tp), when)

    def arrived(owner):
        remote(y, yfull.at[rows_of(owner)], ysend.at[0], yrecv.at[owner], g.kv, g.tp).wait_recv()

    def line(z, other):
        owner = z * SIDE + g.y
        arrived(owner)
        src = yfull.at[rows_of(owner)]
        if other is not None:
            put(src, owner, other, g.y, g.mid)
        put(src, owner, g.z, oy)

    def t_copy(i, step):
        rows = rows_of(order[i], SIDE)
        return remote(
            part.at[rows, lanes(g.t(step))], got.at[step - 1, rows],
            tsend.at[0], trecv.at[0], g.kv, g.t(step),
        )

    order = (g.z, g.z1, g.z3, g.z2)

    def project(i):
        arrived(order[i] * SIDE + oy)
        rows = rows_of(order[i], SIDE)
        part[rows, :] = jnp.dot(yfull[rows, :], po[...], preferred_element_type=F32).astype(BF16)
        for step in range(1, nt):
            t_copy(i, step).start()

    with jax.named_scope("ygather"):
        put(y, g.kv, g.z1, g.y)
        put(y, g.kv, g.z3, g.y)
        put(y, g.kv, g.z, oy)
        yfull[rows_of(g.kv), :] = y[...]
        po_load[0].wait()
        line(g.z1, g.z3)
        line(g.z3, g.z1)
        project(0)
        line(g.z2, None)
        for i in range(1, LINE):
            project(i)
    with jax.named_scope("tscatter"):
        total = part[:, lanes(g.tp)].astype(F32)
        block_ff.send_down()
        drain(got, trecv.at[0])
        for step in range(1, nt):
            total = total + got[step - 1].astype(F32)
        second[...] = (first[...].astype(F32) + total).astype(BF16)
    result[...] = block_ff.run(second).astype(BF16)
    block_ff.finish()
    drain(got, tsend.at[0])
    pl.when(g.mid)(lambda: drain(yfull, ysend.at[0]))
    pl.when(jnp.logical_not(g.mid))(lambda: drain(yfull.at[: (nk - 2) * own_rows], ysend.at[0]))


def call(kernel, ident, outs, n_vmem, n_any, scratch, args):
    vmem, any_space = pl.BlockSpec(memory_space=pltpu.VMEM), pl.BlockSpec(memory_space=pl.ANY)
    return pl.pallas_call(
        kernel,
        out_shape=outs,
        in_specs=[vmem] * n_vmem + [any_space] * n_any,
        out_specs=jax.tree.map(lambda _: vmem, outs),
        scratch_shapes=scratch,
        cost_estimate=pl.CostEstimate(flops=50_000_000_000, bytes_accessed=1, transcendentals=0),
        compiler_params=pltpu.CompilerParams(
            collective_id=ident, has_side_effects=True, vmem_limit_bytes=34 * 1024 * 1024
        ),
    )(*args[:n_vmem], *[pltpu.with_memory_space_constraint(a, pltpu.HBM) for a in args[n_vmem:]])


def per_device(
    tokens, past_state, pre_gain, pre_gate, pre_up, pre_down, mix_gain,
    query_weight, forget_weight, value_weight, output_gate_weight,
    forget_floor, head_gain, proj_out, post_gain, post_gate, post_up, post_down,
):
    nk, nt = lax.axis_size("kv"), lax.axis_size("tp")
    rows, depth, units = tokens.shape[0], pre_gate.shape[0], pre_gate.shape[1]
    own_rows, local_heads, head_width = past_state.shape[:3]
    inner = local_heads * head_width
    width = query_weight.shape[0]
    dma = pltpu.SemaphoreType.DMA
    base = ff_scratch(nk, nt, rows, depth, units)
    first, projected = call(
        functools.partial(first_kernel, nk, nt),
        0,
        (jax.ShapeDtypeStruct(tokens.shape, BF16), jax.ShapeDtypeStruct((own_rows, 4 * inner), F32)),
        0,
        10,
        base
        + [
            pltpu.VMEM(tokens.shape, BF16),
            pltpu.VMEM((1, depth), F32),
            pltpu.VMEM((1, depth), F32),
            dma((3,)),
            pltpu.VMEM((4, width, inner), BF16),
            dma((4,)),
            pltpu.VMEM((rows, width), BF16),
            dma((1,)),
            dma((nt, 2)),
            pltpu.VMEM((rows, width), BF16),
            pltpu.VMEM((rows, 4 * inner), BF16),
            pltpu.VMEM((LINE, 2, own_rows, 2 * inner), BF16),
            pltpu.VMEM((2, 2, own_rows, 2 * inner), BF16),
            pltpu.VMEM((2, 2, own_rows, 2 * inner), BF16),
            pltpu.VMEM((2, own_rows, 2 * inner), BF16),
            pltpu.VMEM((2, own_rows, 2 * inner), BF16),
            pltpu.VMEM((8, rows), F32),
            pltpu.VMEM((nk - 1, 8, LANES), F32),
            pltpu.VMEM((LANES, LANES), F32),
            dma((1,)),
            dma((LINE, 2)),
            dma((1,)),
            dma((2, 2)),
            dma((1,)),
            dma((2,)),
            dma((1,)),
            dma((1,)),
        ],
        (
            tokens, pre_gain[None], mix_gain[None], pre_gate.T, pre_up.T, pre_down,
            query_weight, forget_weight, value_weight, output_gate_weight,
        ),
    )
    new_state, mixed_in = recurrence(projected, past_state, forget_floor, head_gain)
    result = call(
        functools.partial(second_kernel, nk, nt),
        1,
        jax.ShapeDtypeStruct(tokens.shape, BF16),
        3,
        4,
        base
        + [
            pltpu.VMEM(proj_out.shape, BF16),
            dma((1,)),
            pltpu.VMEM((rows, inner), BF16),
            dma((1,)),
            dma((nk,)),
            pltpu.VMEM((rows, width), BF16),
            pltpu.VMEM((nt - 1, rows, LANES), BF16),
            dma((1,)),
            dma((1,)),
            pltpu.VMEM((rows, LANES), BF16),
        ],
        (mixed_in, first, post_gain[None], proj_out, post_gate.T, post_up.T, post_down),
    )
    return (result, new_state)


def solution(mesh):
    placed = (
        P(None, ("kv", "tp")),
        P("kv", "tp", None, None),
        P(),
        P(None, ("kv", "tp")),
        P(None, ("kv", "tp")),
        P(("kv", "tp"), None),
        P(),
        P("kv", "tp"),
        P("kv", "tp"),
        P("kv", "tp"),
        P("kv", "tp"),
        P("tp"),
        P(),
        P("tp", "kv"),
        P(),
        P(None, ("kv", "tp")),
        P(None, ("kv", "tp")),
        P(("kv", "tp"), None),
    )
    blocks_fit = D == mesh.shape["kv"] * mesh.shape["tp"] * LANES and mesh.shape["tp"] == SIDE * CORES and mesh.shape["kv"] == LINE * SIDE
    return jax.shard_map(
        per_device if blocks_fit else per_device_plain,
        mesh=mesh,
        in_specs=placed,
        out_specs=(P(None, ("kv", "tp")), P("kv", "tp", None, None)),
        check_vma=False,
    )
```

time: 132 us -> 112 us (0.85)
  Pallas kernels: 125 us -> 110 us
  local copies, waits for them, and re-layouts: 6.42 us -> 0.66 us
    pallas_call x2, Pallas kernels: 114 us -> 105 us  [call(): pl.pallas_call(kernel, out_shape=outs, in_specs=[vmem] * n_vmem + [any_sp...]
    pallas_call x1, Pallas kernels: 10.7 us -> 4.74 us  [recurrence(): pl.pallas_call(recurrence_kernel, grid=(rows // step,), out_shape=(jax.Sh...]
    unnamed x11, local copies, waits for them, and re-layouts: 6.42 us -> 0.66 us
where the time goes in v2:
time: 112 us
  Pallas kernels  110 us (98%)
    pallas_call x2, Pallas kernels, call(): pl.pallas_call(kernel, out_shape=outs, in_specs=[vmem] * n_vmem + [any_sp...  105 us
    pallas_call x1, Pallas kernels, recurrence(): pl.pallas_call(recurrence_kernel, grid=(rows // step,), out_shape=(jax.Sh...  4.74 us

profile of v2, /device:TPU:0, one launch (start us, length us, event | category | flops | bytes accessed | tf_op | source)
XLA Modules:
  0.0 111.6 jit_solution(12882833579822546201)
XLA Ops:
  0.6 0.0 slice-start
  0.6 0.0 slice-start.1
  0.7 0.0 copy-start
  0.7 0.0 copy-start.1
  0.7 58.4 %shard_map.185 = (bf16[256,128]{1,0:T(8,128)(2,1)S(1)}, f32[32,2048]{1,0:T(8,128)S(1)}) custom-call(bf16[256,128]{1,0:T(8,128)(2,1)} %tok_h.1, f32[1,4096]{1,0:T(1,128)} %bitcast.18, f32[1,4096]{1,0:T(1,128)} %bitcast.19, bf16[352,4096]{1,0:T(8,128)(2,1)} %bitcast.14, bf16[352,4096]{1,0:T(8,128)(2,1)} %bitcast.15, bf16[352,4096]{1,0:T(8,128)(2,1)} %wd_h.2, ...), custom_call_target="tpu_custom_call" | custom-call | flops 49999998976 | bytes 1 | tf_op jit(solution)/shard_map/pallas_call | solution.py:788
  59.1 0.0 slice-done
  59.1 0.0 slice-done.1
  59.1 0.0 copy-done
  59.1 0.0 copy-done.1
  59.1 0.0 copy-start.2
  59.2 4.7 %shard_map.186 = (f32[32,4,128,128]{3,2,1,0:T(8,128)}, bf16[32,512]{1,0:T(8,128)(2,1)S(1)}) custom-call(f32[32,2048]{1,0:T(8,128)S(1)} %get-tuple-element.6.projected, f32[32,4,128,128]{3,2,1,0:T(8,128)S(1)} %bitcast.10, f32[1,512]{1,0:T(1,128)S(1)} %bitcast.11, f32[1,128]{1,0:T(1,128)S(1)} %bitcast.12), custom_call_target="tpu_custom_call" | custom-call | tf_op jit(solution)/shard_map/pallas_call | solution.py:694
  63.9 0.0 copy-done.2
  63.9 47.1 %shard_map.187 = bf16[256,128]{1,0:T(8,128)(2,1)S(1)} custom-call(bf16[32,512]{1,0:T(8,128)(2,1)S(1)} %get-tuple-element.7.y, bf16[256,128]{1,0:T(8,128)(2,1)S(1)} %get-tuple-element.8.first, f32[1,4096]{1,0:T(1,128)S(1)} %bitcast.13, bf16[512,512]{1,0:T(8,128)(2,1)} %po_h.1, bf16[352,4096]{1,0:T(8,128)(2,1)} %bitcast.16, bf16[352,4096]{1,0:T(8,128)(2,1)} %bitcast.17, ...), custom_call_target="tpu_custom_call" | custom-call | flops 49999998976 | bytes 1 | tf_op jit(solution)/shard_map/pallas_call | solution.py:788
  111.0 0.6 copy.21
  (1 shorter events, 0.0 us)
Async XLA Ops:
  0.6 58.5 %slice-start = ((s8[8388608]{0:T(1024)(128)(4,1)}), s8[4194304]{0:T(1024)(128)(4,1)S(1)}, s32[]{:S(2)}) async-start(s8[8388608]{0:T(1024)(128)(4,1)} %bitcast.9), calls=%async_computation | async-start | bytes 8388608
  0.6 58.5 %slice-start.1 = ((s8[8388608]{0:T(1024)(128)(4,1)}), s8[4194304]{0:T(1024)(128)(4,1)S(1)}, s32[]{:S(2)}) async-start(s8[8388608]{0:T(1024)(128)(4,1)} %bitcast.9), calls=%async_computation.1 | async-start | bytes 8388608
  0.7 58.5 %copy-start = (f32[512]{0:T(512)S(1)}, f32[512]{0:T(512)}, u32[]{:S(2)}) copy-start(f32[512]{0:T(512)} %param.29) | copy-start | bytes 6148
  0.7 58.5 %copy-start.1 = (f32[128]{0:T(128)S(1)}, f32[128]{0:T(128)}, u32[]{:S(2)}) copy-start(f32[128]{0:T(128)} %param.30) | copy-start | bytes 1540
  59.1 4.8 %copy-start.2 = (f32[4096]{0:T(1024)S(1)}, f32[4096]{0:T(1024)}, u32[]{:S(2)}) copy-start(f32[4096]{0:T(1024)} %param.32) | copy-start | bytes 49156
